TPU v7x, 32 devices: a whole 2x2x4 slice. The times are simulated.
32 devices in a mesh: sp: 8 (over z, y), tp: 4 (over x, core).
Axes of the slice: x: 2, y: 2, z: 4, core: 2. Of those that a mesh axis runs over, the one named last changes fastest.
Arguments:
- resid: bfloat16 [1536, 2048], P('sp'), may hold values from -6 to 6
- query_broad: bfloat16 [1536, 1536], P('sp', 'tp'), may hold values from -60 to 60
- query_narrow: bfloat16 [1536, 1024], P('sp', 'tp'), may hold values from -60 to 60
- latent: bfloat16 [1536, 512], P('sp'), may hold values from -6 to 6
- key_rope: bfloat16 [1536, 64], P('sp'), may hold values from -6 to 6
- latent_gain: float32 [512], replicated, may hold values from 0.1 to 1.9
- key_up_broad: bfloat16 [512, 1024], P(None, 'tp'), may hold values from -0.25 to 0.25
- value_up_broad: bfloat16 [512, 1024], P(None, 'tp'), may hold values from -0.25 to 0.25
- key_up_narrow: bfloat16 [512, 512], P(None, 'tp'), may hold values from -0.25 to 0.25
- value_up_narrow: bfloat16 [512, 512], P(None, 'tp'), may hold values from -0.25 to 0.25
- out_broad: bfloat16 [1024, 2048], replicated, may hold values from -0.15625 to 0.15625
- out_narrow: bfloat16 [512, 2048], replicated, may hold values from -0.15625 to 0.15625
- post_gain: float32 [2048], replicated, may hold values from 0.1 to 1.9
- ffn_gain: float32 [2048], replicated, may hold values from 0.1 to 1.9
- up_weight: bfloat16 [2048, 8192], P('sp', 'tp'), may hold values from -0.125 to 0.125
- down_weight: bfloat16 [2048, 8192], P('sp', 'tp'), may hold values from -0.0625 to 0.0625
- ffn_out_gain: float32 [2048], replicated, may hold values from 0.1 to 1.9
Outputs:
- layer_out: bfloat16 [1536, 2048], P(('sp', 'tp'))
All inputs are finite; a program needn't handle non-finite values.
Results may differ from a plain program's by a relative error of at most 0.013.
Values may be sent and summed in bfloat16 or wider, within the bound.
A program may use at most 128 MiB of HBM per device.

v0:
```python
import functools
import math

import jax
import jax.numpy as jnp
from jax import lax
from jax.experimental import pallas as pl
from jax.experimental.pallas import tpu as pltpu
from jax.sharding import PartitionSpec as P

DB = 128
DN = 64


norm_eps = 1e-06
rope_base = 500000.0
masked_score = -1e30


def rotate(values, positions):
    full_width = values.shape[-1]
    half_width = full_width // 2
    frequency = rope_base ** (-2.0 * jnp.arange(half_width, dtype=jnp.float32) / full_width)
    angles = positions.astype(jnp.float32)[:, None] * frequency[None, :]
    angle_shape = (angles.shape[0],) + (1,) * (values.ndim - 2) + (half_width,)
    cosine = jnp.cos(angles).reshape(angle_shape)
    sine_part = jnp.sin(angles).reshape(angle_shape)
    leading = values[..., :half_width]
    trailing = values[..., half_width:]
    return jnp.concatenate(
        [leading * cosine - trailing * sine_part, trailing * cosine + leading * sine_part], axis=-1
    )


def rms_scale(values, norm_gain):
    return (
        values * lax.rsqrt(jnp.mean(values * values, axis=-1, keepdims=True) + norm_eps) * norm_gain
    )


def group_update(
    running, nope_query, rope_query, key_rows, key_rot, value_rows, score_scale, allowed
):
    old_max, old_sum, old_acc = running
    scores = jnp.einsum("qhd,khd->hqk", nope_query, key_rows, preferred_element_type=jnp.float32)
    scores = scores + jnp.einsum(
        "qhd,kd->hqk", rope_query, key_rot, preferred_element_type=jnp.float32
    )
    scores = jnp.where(allowed, scores * score_scale, masked_score)
    new_max = jnp.maximum(old_max, jnp.max(scores, axis=-1))
    exponent = jnp.where(allowed, jnp.exp(scores - new_max[:, :, None]), 0.0)
    factor = jnp.exp(old_max - new_max)
    new_sum = old_sum * factor + jnp.sum(exponent, axis=-1)
    weighted = jnp.einsum(
        "hqk,khd->qhd",
        exponent.astype(jnp.bfloat16),
        value_rows,
        preferred_element_type=jnp.float32,
    )
    new_acc = old_acc * jnp.transpose(factor)[:, :, None] + weighted
    return (new_max, new_sum, new_acc)


def local(
    resid,
    query_broad,
    query_narrow,
    latent,
    key_rope,
    latent_gain,
    key_up_broad,
    value_up_broad,
    key_up_narrow,
    value_up_narrow,
    out_broad,
    out_narrow,
    post_gain,
    ffn_gain,
    up_weight,
    down_weight,
    ffn_out_gain,
):
    local_rows = resid.shape[0]
    head_parts = lax.axis_size("tp")
    share_rows = local_rows // head_parts
    row_offset = lax.axis_index("sp") * local_rows
    last_query = row_offset + local_rows - 1
    query_pos = row_offset + jnp.arange(local_rows, dtype=jnp.int32)
    rope_width = key_rope.shape[1]
    broad_count = key_up_broad.shape[1] // DB
    narrow_count = key_up_narrow.shape[1] // DN
    broad_heads = query_broad.reshape(local_rows, broad_count, DB + rope_width)
    broad_nope = broad_heads[:, :, :DB]
    broad_rope = rotate(broad_heads[:, :, DB:].astype(jnp.float32), query_pos).astype(jnp.bfloat16)
    narrow_heads = query_narrow.reshape(local_rows, narrow_count, DN + rope_width)
    narrow_nope = narrow_heads[:, :, :DN]
    narrow_rope = rotate(narrow_heads[:, :, DN:].astype(jnp.float32), query_pos).astype(
        jnp.bfloat16
    )
    broad_scale = (DB + rope_width) ** (-0.5)
    narrow_scale = (DN + rope_width) ** (-0.5)

    def attend(running, latent_rows, rope_rows, first_row):
        key_count = latent_rows.shape[0]
        key_pos = first_row + jnp.arange(key_count, dtype=jnp.int32)
        latent_normed = rms_scale(latent_rows.astype(jnp.float32), latent_gain).astype(jnp.bfloat16)

        def expand(weight, head_size):
            product = jnp.dot(latent_normed, weight, preferred_element_type=jnp.float32)
            return product.astype(jnp.bfloat16).reshape(key_count, -1, head_size)

        key_rot = rotate(rope_rows.astype(jnp.float32), key_pos).astype(jnp.bfloat16)
        allowed = (key_pos[None, :] <= query_pos[:, None])[None]
        broad_state = group_update(
            running[0],
            broad_nope,
            broad_rope,
            expand(key_up_broad, DB),
            key_rot,
            expand(value_up_broad, DB),
            broad_scale,
            allowed,
        )
        narrow_state = group_update(
            running[1],
            narrow_nope,
            narrow_rope,
            expand(key_up_narrow, DN),
            key_rot,
            expand(value_up_narrow, DN),
            narrow_scale,
            allowed,
        )
        return (broad_state, narrow_state)

    def fresh(head_count, head_size):
        return (
            jnp.full((head_count, local_rows), masked_score, jnp.float32),
            jnp.zeros((head_count, local_rows), jnp.float32),
            jnp.zeros((local_rows, head_count, head_size), jnp.float32),
        )

    initial = (fresh(broad_count, DB), fresh(narrow_count, DN))
    latent_piece = lax.all_gather(latent, "sp", axis=0, tiled=True)
    rope_piece = lax.all_gather(key_rope, "sp", axis=0, tiled=True)
    piece_rows = latent_piece.shape[0]
    block_rows = math.gcd(piece_rows, 1024)

    def one_block(block_index, carried):
        begin = block_index * block_rows
        latent_block = lax.dynamic_slice_in_dim(latent_piece, begin, block_rows, 0)
        rope_block = lax.dynamic_slice_in_dim(rope_piece, begin, block_rows, 0)

        def unchanged(kept_state):
            return kept_state

        def updated(kept_state):
            return attend(kept_state, latent_block, rope_block, begin)

        return lax.cond(begin > last_query, unchanged, updated, carried)

    final_state = lax.fori_loop(0, piece_rows // block_rows, one_block, initial)

    def finish(running):
        run_max, run_sum, run_acc = running
        return (
            (run_acc / jnp.transpose(run_sum)[:, :, None])
            .astype(jnp.bfloat16)
            .reshape(local_rows, -1)
        )

    attn_broad = finish(final_state[0])
    attn_narrow = finish(final_state[1])
    rows_broad, rows_narrow = (
        lax.all_to_all(attn_broad, "tp", split_axis=0, concat_axis=1, tiled=True),
        lax.all_to_all(attn_narrow, "tp", split_axis=0, concat_axis=1, tiled=True),
    )
    projected = jnp.dot(rows_broad, out_broad, preferred_element_type=jnp.float32) + jnp.dot(
        rows_narrow, out_narrow, preferred_element_type=jnp.float32
    )
    own_resid = lax.dynamic_slice_in_dim(resid, lax.axis_index("tp") * share_rows, share_rows, 0)
    mixed = (own_resid.astype(jnp.float32) + rms_scale(projected, post_gain)).astype(jnp.bfloat16)
    normed = rms_scale(mixed.astype(jnp.float32), ffn_gain).astype(jnp.bfloat16)
    up_full, down_full = (
        lax.all_gather(up_weight, "sp", axis=0, tiled=True),
        lax.all_gather(down_weight, "sp", axis=0, tiled=True),
    )
    hidden = jnp.square(
        jax.nn.relu(
            jnp.dot(
                lax.all_gather(normed, "tp", axis=0, tiled=True),
                up_full,
                preferred_element_type=jnp.float32,
            )
        )
    ).astype(jnp.bfloat16)
    ffn = lax.psum_scatter(
        lax.dot_general(
            hidden, down_full, (((1,), (1,)), ((), ())), preferred_element_type=jnp.float32
        ).astype(jnp.bfloat16),
        "tp",
        scatter_dimension=0,
        tiled=True,
    ).astype(jnp.float32)
    return (mixed.astype(jnp.float32) + rms_scale(ffn, ffn_out_gain)).astype(jnp.bfloat16)

lane_tile = 128
row_parts = 2


def attend_rows(qb_ref, qn_ref, lat_ref, kb_ref, vb_ref, kn_ref, vn_ref, o_ref):
    rows = qb_ref.shape[0]
    latent_width = kb_ref.shape[0]
    rope = lat_ref.shape[3] - latent_width
    share = o_ref.shape[1]
    block = 2 * rows
    broad = kb_ref.shape[1] // DB
    narrow = kn_ref.shape[1] // DN
    first = lax.axis_index("sp") * rows
    blocks = lax.div(first + rows + block - 1, block)
    query_pos = first + lax.broadcasted_iota(jnp.int32, (rows, block), 0)
    key_iota = lax.broadcasted_iota(jnp.int32, (rows, block), 1)
    wb = DB + rope
    wn = DN + rope
    heads = broad + narrow
    widths = [DB] * broad + [narrow * DN] * narrow

    def step(index, carried):
        start = pl.multiple_of(index * block, block)
        both = lat_ref[pl.ds(2 * index, 2)].reshape(block, latent_width + rope)
        lat = both[:, :latent_width]
        rot = both[:, latent_width:]

        def expand(ref):
            return jnp.dot(lat, ref[...], preferred_element_type=jnp.float32).astype(jnp.bfloat16)

        kb, vb, kn, vn = expand(kb_ref), expand(vb_ref), expand(kn_ref), expand(vn_ref)
        allowed = key_iota + start <= query_pos
        out = []
        for h in range(heads):
            old_max, old_sum, old_acc = carried[h]
            if h < broad:
                q = qb_ref[:, h * wb : (h + 1) * wb]
                k = jnp.concatenate([kb[:, h * DB : (h + 1) * DB], rot], axis=1)
                v = vb[:, h * DB : (h + 1) * DB]
                scale = wb ** (-0.5)
            else:
                n = h - broad
                q = qn_ref[:, n * wn : (n + 1) * wn]
                k = jnp.concatenate([kn[:, n * DN : (n + 1) * DN], rot], axis=1)
                v = vn
                scale = wn ** (-0.5)
            s = lax.dot_general(
                q, k, (((1,), (1,)), ((), ())), preferred_element_type=jnp.float32
            )
            s = jnp.where(allowed, s * scale, masked_score)
            new_max = jnp.maximum(old_max, jnp.max(s, axis=-1, keepdims=True))
            e = jnp.where(allowed, jnp.exp(s - new_max), 0.0)
            factor = jnp.exp(old_max - new_max)
            new_sum = old_sum * factor + jnp.sum(e, axis=-1, keepdims=True)
            pv = jnp.dot(e.astype(jnp.bfloat16), v, preferred_element_type=jnp.float32)
            out.append((new_max, new_sum, old_acc * factor + pv))
        return tuple(out)

    init = tuple(
        (
            jnp.full((rows, 1), masked_score, jnp.float32),
            jnp.zeros((rows, 1), jnp.float32),
            jnp.zeros((rows, w), jnp.float32),
        )
        for w in widths
    )
    final = lax.fori_loop(0, blocks, step, init)
    parts = [final[h][2] / final[h][1] for h in range(heads)]
    for h in range(broad):
        for t in range(o_ref.shape[0]):
            o_ref[t, :, h * DB : (h + 1) * DB] = parts[h][t * share : (t + 1) * share].astype(
                o_ref.dtype
            )
    if narrow:
        column = lax.broadcasted_iota(jnp.int32, parts[broad].shape, 1)
        mixed = parts[broad]
        for n in range(1, narrow):
            mixed = jnp.where(column >= n * DN, parts[broad + n], mixed)
        for t in range(o_ref.shape[0]):
            o_ref[t, :, broad * DB :] = mixed[t * share : (t + 1) * share].astype(o_ref.dtype)


def layer_kernel(
    sp,
    tp,
    latent_ref,
    key_rope_ref,
    table_ref,
    latent_gain_ref,
    qb_in,
    qn_in,
    resid_ref,
    kb_ref,
    vb_ref,
    kn_ref,
    vn_ref,
    ob_hbm,
    on_hbm,
    post_ref,
    gain_ref,
    last_ref,
    up_hbm,
    down_hbm,
    out_ref,
    mine_ref,
    qb_ref,
    qn_ref,
    lat,
    attn,
    heads,
    ob,
    on,
    up,
    down,
    rows,
    total,
    core_send,
    core_got,
    x_send,
    x_got,
    z_send,
    z_got,
    send_sem,
    recv_sem,
    local_sem,
):
    cols = row_parts
    lines = sp // cols
    s = lax.axis_index("sp")
    t = lax.axis_index("tp")
    z = s // cols
    y = s % cols
    core = t % 2
    ports = t // 2
    t_core = t + 1 - 2 * core
    t_x = (1 - ports) * 2 + core
    t_both = (1 - ports) * 2 + (1 - core)
    s_y = z * cols + 1 - y
    bf16 = jnp.bfloat16
    share = resid_ref.shape[0] // tp
    width = up.shape[2]

    def line(k):
        return (z + k + lines) % lines * cols + y

    def source(k, flipped):
        return (z - k + lines) % lines * cols + ((1 - y) if flipped else y)

    peers = [(line(k), t) for k in range(1, lines)]
    peers += [(s_y, t), (s, t_core), (s, t_x), (s, t_both)]
    barrier = pltpu.get_barrier_semaphore()
    for peer in peers:
        pl.semaphore_signal(
            barrier, inc=1, device_id=peer, device_id_type=pl.DeviceIdType.MESH
        )

    rope = key_rope_ref.shape[1]
    half_rope = rope // 2

    def turn(values, table):
        values = values.astype(jnp.float32)
        swapped = jnp.concatenate([values[:, half_rope:], values[:, :half_rope]], axis=1)
        return (values * table[:, :rope] + swapped * table[:, rope:]).astype(bf16)

    latent_width = latent_ref.shape[1]
    half = mine_ref.shape[0]
    mine_rows = pl.ds(pl.multiple_of(core * half, 16), half)
    mine_ref[:, :latent_width] = rms_scale(
        latent_ref[mine_rows, :].astype(jnp.float32), latent_gain_ref[...]
    ).astype(bf16)
    mine_ref[:, latent_width:] = turn(key_rope_ref[mine_rows, :], table_ref[mine_rows, :])
    pl.semaphore_wait(barrier, len(peers))

    started = []

    def send(src, dst, peer):
        i = len(started)
        copy = pltpu.make_async_remote_copy(
            src_ref=src,
            dst_ref=dst,
            send_sem=send_sem.at[i],
            recv_sem=recv_sem.at[i],
            device_id=peer,
            device_id_type=pl.DeviceIdType.MESH,
        )
        copy.start()
        started.append(copy)
        return copy

    locals_ = []

    def bring(src, dst):
        copy = pltpu.make_async_copy(src, dst, local_sem.at[len(locals_)])
        copy.start()
        locals_.append(copy)
        return copy

    def cut(ref, k):
        at = pl.multiple_of((z + k) % lines * width, width)
        return ref.at[:, pl.ds(at, width)]

    far = list(range(1, lines))
    lat_z = {k: send(mine_ref, lat.at[s, core], (line(k), t)) for k in far}
    lat_y = {0: send(mine_ref, lat.at[s, core], (s_y, t))}
    lat_c = [send(mine_ref, lat.at[s, core], (s, t_core))]
    up_z = {k: send(cut(up_hbm, k), up.at[s], (line(k), t)) for k in far}
    down_z = {k: send(cut(down_hbm, k), down.at[s], (line(k), t)) for k in far}
    own = [bring(cut(up_hbm, 0), up.at[s]), bring(cut(down_hbm, 0), down.at[s])]
    outs = [bring(ob_hbm, ob), bring(on_hbm, on)]
    lat[s, core] = mine_ref[...]
    for queries, turned, size in ((qb_in, qb_ref, DB), (qn_in, qn_ref, DN)):
        step = size + rope
        for h in range(queries.shape[1] // step):
            middle = h * step + size
            turned[:, h * step : middle] = queries[:, h * step : middle]
            turned[:, middle : middle + rope] = turn(
                queries[:, middle : middle + rope], table_ref[...]
            )
    order = sorted(far, key=lambda k: min(k, lines - k))
    for k in order:
        lat_z[k].wait_recv()
        held = lat.at[source(k, False), core]
        lat_y[k] = send(held, held, (s_y, t))
        lat_c.append(send(held, held, (s, t_core)))
    for k in [0] + order:
        lat_y[k].wait_recv()
        held = lat.at[source(k, True), core]
        lat_c.append(send(held, held, (s, t_core)))
    up_y = [send(cut(up_hbm, 0), up.at[s], (s_y, t))]
    down_y = [send(cut(down_hbm, 0), down.at[s], (s_y, t))]
    for copy in lat_c:
        copy.wait_recv()

    attend_rows(qb_ref, qn_ref, lat, kb_ref, vb_ref, kn_ref, vn_ref, attn)

    moved = [
        send(attn.at[peer], heads.at[t], (s, peer)) for peer in (t_x, t_both, t_core)
    ]
    heads[t] = attn[t]
    for k in order:
        up_z[k].wait_recv()
        held = up.at[source(k, False)]
        up_y.append(send(held, held, (s_y, t)))
    for copy in outs:
        copy.wait()
    for copy in moved:
        copy.wait_recv()

    broad_width = kb_ref.shape[1]
    narrow_width = kn_ref.shape[1]
    projected = jnp.zeros((share, ob.shape[1]), jnp.float32)
    for i in range(tp):
        projected = projected + jnp.dot(
            heads[i, :, :broad_width],
            ob[i * broad_width : (i + 1) * broad_width],
            preferred_element_type=jnp.float32,
        )
        projected = projected + jnp.dot(
            heads[i, :, broad_width:],
            on[i * narrow_width : (i + 1) * narrow_width],
            preferred_element_type=jnp.float32,
        )
    mixed = (
        resid_ref[pl.ds(pl.multiple_of(t * share, 16), share), :].astype(jnp.float32)
        + rms_scale(projected, post_ref[...])
    ).astype(bf16)
    rows[0, 0] = rms_scale(mixed.astype(jnp.float32), gain_ref[...]).astype(bf16)

    row_z = {k: send(rows.at[0, 0], rows.at[0, k], (line(k), t)) for k in far}
    row_x = {0: send(rows.at[0, 0], rows.at[1, 0], (s, t_x))}
    row_c = {0: send(rows.at[0, 0], rows.at[2, 0], (s, t_core))}
    row_b = {}
    for k in order:
        down_z[k].wait_recv()
        held = down.at[source(k, False)]
        down_y.append(send(held, held, (s_y, t)))
    row_x[0].wait_recv()
    row_b[0] = send(rows.at[1, 0], rows.at[3, 0], (s, t_core))
    for k in order:
        row_z[k].wait_recv()
        row_x[k] = send(rows.at[0, k], rows.at[1, k], (s, t_x))
        row_c[k] = send(rows.at[0, k], rows.at[2, k], (s, t_core))
    for copy in own:
        copy.wait()
    for copy in up_y + down_y:
        copy.wait_recv()

    deep = sp * up.shape[1]

    def feed(j):
        block = rows[j].reshape(lines * share, rows.shape[3])
        product = jnp.dot(block, up[...].reshape(deep, width), preferred_element_type=jnp.float32)
        hidden = jnp.square(jnp.maximum(product, 0.0)).astype(bf16)
        return lax.dot_general(
            hidden,
            down[...].reshape(deep, width),
            (((1,), (1,)), ((), ())),
            preferred_element_type=jnp.float32,
        )

    total[0] = feed(0)
    for k in [0] + order:
        row_c[k].wait_recv()
    core_send[0] = feed(2).astype(bf16)
    sum_c = [send(core_send.at[0], core_got.at[0], (s, t_core))]
    for k in order:
        row_x[k].wait_recv()
        row_b[k] = send(rows.at[1, k], rows.at[3, k], (s, t_core))
    total[1] = feed(1)
    for k in [0] + order:
        row_b[k].wait_recv()
    core_send[1] = feed(3).astype(bf16)
    sum_c.append(send(core_send.at[1], core_got.at[1], (s, t_core)))
    sum_c[1].wait_recv()
    sum_x = {}
    back = order[::-1] + [0]
    for k in back:
        part = slice(k * share, (k + 1) * share)
        x_send[k] = (total[1, part] + core_got[1, part].astype(jnp.float32)).astype(bf16)
        sum_x[k] = send(x_send.at[k], x_got.at[k], (s, t_x))
    sum_c[0].wait_recv()
    sum_z = []
    for k in back:
        part = slice(k * share, (k + 1) * share)
        sum_x[k].wait_recv()
        piece = (
            total[0, part]
            + core_got[0, part].astype(jnp.float32)
            + x_got[k].astype(jnp.float32)
        )
        if k:
            z_send[k] = piece.astype(bf16)
            sum_z.append(send(z_send.at[k], z_got.at[k], (line(-k), t)))
        else:
            ffn = piece
    for copy in sum_z:
        copy.wait_recv()
    for k in far:
        ffn = ffn + z_got[k].astype(jnp.float32)
    out_ref[...] = (mixed.astype(jnp.float32) + rms_scale(ffn, last_ref[...])).astype(bf16)
    for copy in started:
        copy.wait_send()


def fast_local(
    resid,
    query_broad,
    query_narrow,
    latent,
    key_rope,
    latent_gain,
    key_up_broad,
    value_up_broad,
    key_up_narrow,
    value_up_narrow,
    out_broad,
    out_narrow,
    post_gain,
    ffn_gain,
    up_weight,
    down_weight,
    ffn_out_gain,
):
    sp = lax.axis_size("sp")
    tp = lax.axis_size("tp")
    cols = row_parts
    lines = sp // cols
    s = lax.axis_index("sp")
    z = s // cols
    y = s % cols
    local_rows = resid.shape[0]
    share_rows = local_rows // tp
    query_pos = s * local_rows + jnp.arange(local_rows, dtype=jnp.int32)
    rope_width = key_rope.shape[1]
    bf16 = jnp.bfloat16

    frequency = rope_base ** (-2.0 * jnp.arange(rope_width // 2, dtype=jnp.float32) / rope_width)
    angles = query_pos.astype(jnp.float32)[:, None] * frequency[None, :]
    cosine, sine = jnp.cos(angles), jnp.sin(angles)
    table = jnp.concatenate([cosine, cosine, -sine, sine], axis=1)
    half_rows = local_rows // 2
    both_width = latent.shape[1] + rope_width
    broad_width = key_up_broad.shape[1]
    narrow_width = key_up_narrow.shape[1]
    width = broad_width + narrow_width
    deep = resid.shape[1]
    slice_width = up_weight.shape[1] // lines
    vmem = pl.BlockSpec(memory_space=pltpu.VMEM)
    anywhere = pl.BlockSpec(memory_space=pl.ANY)
    return pl.pallas_call(
        functools.partial(layer_kernel, sp, tp),
        out_shape=jax.ShapeDtypeStruct((share_rows, deep), bf16),
        in_specs=[vmem] * 11 + [anywhere] * 2 + [vmem] * 3 + [anywhere] * 2,
        out_specs=vmem,
        scratch_shapes=[
            pltpu.VMEM((half_rows, both_width), bf16),
            pltpu.VMEM(query_broad.shape, bf16),
            pltpu.VMEM(query_narrow.shape, bf16),
            pltpu.VMEM((sp, 2, half_rows, both_width), bf16),
            pltpu.VMEM((tp, share_rows, width), bf16),
            pltpu.VMEM((tp, share_rows, width), bf16),
            pltpu.VMEM(out_broad.shape, bf16),
            pltpu.VMEM(out_narrow.shape, bf16),
            pltpu.VMEM((sp, up_weight.shape[0], slice_width), bf16),
            pltpu.VMEM((sp, up_weight.shape[0], slice_width), bf16),
            pltpu.VMEM((tp, lines, share_rows, deep), bf16),
            pltpu.VMEM((2, lines * share_rows, deep), jnp.float32),
            pltpu.VMEM((2, lines * share_rows, deep), bf16),
            pltpu.VMEM((2, lines * share_rows, deep), bf16),
            pltpu.VMEM((lines, share_rows, deep), bf16),
            pltpu.VMEM((lines, share_rows, deep), bf16),
            pltpu.VMEM((lines, share_rows, deep), bf16),
            pltpu.VMEM((lines, share_rows, deep), bf16),
            pltpu.SemaphoreType.DMA((15 * lines + 2,)),
            pltpu.SemaphoreType.DMA((15 * lines + 2,)),
            pltpu.SemaphoreType.DMA((4,)),
        ],
        compiler_params=pltpu.CompilerParams(
            collective_id=0, has_side_effects=True, vmem_limit_bytes=60 * 2**20
        ),
    )(
        latent,
        key_rope,
        table,
        latent_gain[None],
        query_broad,
        query_narrow,
        resid,
        key_up_broad,
        value_up_broad,
        key_up_narrow,
        value_up_narrow,
        out_broad,
        out_narrow,
        post_gain[None],
        ffn_gain[None],
        ffn_out_gain[None],
        up_weight,
        down_weight,
    )


def solution(mesh):
    in_specs = (
        P("sp", None),
        P("sp", "tp"),
        P("sp", "tp"),
        P("sp", None),
        P("sp", None),
        P(),
        P(None, "tp"),
        P(None, "tp"),
        P(None, "tp"),
        P(None, "tp"),
        P(),
        P(),
        P(),
        P(),
        P("sp", "tp"),
        P("sp", "tp"),
        P(),
    )
    out_specs = P(("sp", "tp"), None)
    sp = mesh.shape["sp"]
    tp = mesh.shape["tp"]

    def whole(*args):
        hidden = args[14].shape[1] // tp
        rows = args[0].shape[0] // sp
        lines = sp // row_parts
        fits = (
            sp % row_parts == 0
            and tp & (tp - 1) == 0
            and tp == 4
            and lines > 1
            and hidden % (lines * lane_tile) == 0
            and rows % (16 * tp) == 0
        )
        body = fast_local if fits else local
        return jax.shard_map(
            body, mesh=mesh, in_specs=in_specs, out_specs=out_specs, check_vma=False
        )(*args)

    return whole
```

profile of v0, /device:TPU:0, one launch (start us, length us, event | category | flops | bytes accessed | tf_op | source)
XLA Modules:
  0.0 122.5 jit_solution(2693479296884755846)
XLA Ops:
  0.0 0.4 multiply_cosine_fusion
  0.4 0.8 pad_maximum_fusion.table_ref
  1.2 1.5 %copy.20.key_rope_ref = bf16[192,64]{1,0:T(8,128)(2,1)} copy(bf16[192,64]{0,1:T(8,128)(2,1)} %param.21) | data formatting | bytes 49152 | tf_op args[4]
  2.7 118.1 %shard_map.163 = bf16[48,2048]{1,0:T(8,128)(2,1)} custom-call(bf16[192,512]{1,0:T(8,128)(2,1)} %latent_ref.1, bf16[192,64]{1,0:T(8,128)(2,1)} %copy.20.key_rope_ref, f32[192,128]{1,0:T(8,128)} %pad_maximum_fusion.table_ref, f32[1,512]{1,0:T(1,128)} %bitcast.7, bf16[192,384]{1,0:T(8,128)(2,1)} %qb_in.1, bf16[192,256]{1,0:T(8,128)(2,1)} %qn_in.1, ...), custom_call_target="tpu_custom_call" | custom-call | tf_op jit(solution)/shard_map/pallas_call | solution.py:596
  120.8 1.6 %copy.22 = bf16[48,2048]{1,0:T(8,128)(2,1)} copy(bf16[48,2048]{1,0:T(8,128)(2,1)} %shard_map.163) | data formatting | bytes 393216
  (2 shorter events, 0.0 us)
where the time goes:
time: 123 us; the launch traced here: 122 us
  Pallas kernels  118 us (96%)
  local copies, waits for them, and re-layouts  3.09 us (3%)
  other arithmetic  1.23 us (1%)
    pallas_call x1, Pallas kernels, fast_local(): pl.pallas_call(functools.partial(layer_kernel, sp, tp), out_shape=jax.Sha...  118 us
    unnamed x2, local copies, waits for them, and re-layouts  3.09 us

commit v1 on v0

v1 whole, which is shorter than its diff:
```python
import functools
import math

import jax
import jax.numpy as jnp
from jax import lax
from jax.experimental import pallas as pl
from jax.experimental.pallas import tpu as pltpu
from jax.sharding import PartitionSpec as P

DB = 128
DN = 64


norm_eps = 1e-06
rope_base = 500000.0
masked_score = -1e30


def rotate(values, positions):
    full_width = values.shape[-1]
    half_width = full_width // 2
    frequency = rope_base ** (-2.0 * jnp.arange(half_width, dtype=jnp.float32) / full_width)
    angles = positions.astype(jnp.float32)[:, None] * frequency[None, :]
    angle_shape = (angles.shape[0],) + (1,) * (values.ndim - 2) + (half_width,)
    cosine = jnp.cos(angles).reshape(angle_shape)
    sine_part = jnp.sin(angles).reshape(angle_shape)
    leading = values[..., :half_width]
    trailing = values[..., half_width:]
    return jnp.concatenate(
        [leading * cosine - trailing * sine_part, trailing * cosine + leading * sine_part], axis=-1
    )


def rms_scale(values, norm_gain):
    return (
        values * lax.rsqrt(jnp.mean(values * values, axis=-1, keepdims=True) + norm_eps) * norm_gain
    )


def group_update(
    running, nope_query, rope_query, key_rows, key_rot, value_rows, score_scale, allowed
):
    old_max, old_sum, old_acc = running
    scores = jnp.einsum("qhd,khd->hqk", nope_query, key_rows, preferred_element_type=jnp.float32)
    scores = scores + jnp.einsum(
        "qhd,kd->hqk", rope_query, key_rot, preferred_element_type=jnp.float32
    )
    scores = jnp.where(allowed, scores * score_scale, masked_score)
    new_max = jnp.maximum(old_max, jnp.max(scores, axis=-1))
    exponent = jnp.where(allowed, jnp.exp(scores - new_max[:, :, None]), 0.0)
    factor = jnp.exp(old_max - new_max)
    new_sum = old_sum * factor + jnp.sum(exponent, axis=-1)
    weighted = jnp.einsum(
        "hqk,khd->qhd",
        exponent.astype(jnp.bfloat16),
        value_rows,
        preferred_element_type=jnp.float32,
    )
    new_acc = old_acc * jnp.transpose(factor)[:, :, None] + weighted
    return (new_max, new_sum, new_acc)


def local(
    resid,
    query_broad,
    query_narrow,
    latent,
    key_rope,
    latent_gain,
    key_up_broad,
    value_up_broad,
    key_up_narrow,
    value_up_narrow,
    out_broad,
    out_narrow,
    post_gain,
    ffn_gain,
    up_weight,
    down_weight,
    ffn_out_gain,
):
    local_rows = resid.shape[0]
    head_parts = lax.axis_size("tp")
    share_rows = local_rows // head_parts
    row_offset = lax.axis_index("sp") * local_rows
    last_query = row_offset + local_rows - 1
    query_pos = row_offset + jnp.arange(local_rows, dtype=jnp.int32)
    rope_width = key_rope.shape[1]
    broad_count = key_up_broad.shape[1] // DB
    narrow_count = key_up_narrow.shape[1] // DN
    broad_heads = query_broad.reshape(local_rows, broad_count, DB + rope_width)
    broad_nope = broad_heads[:, :, :DB]
    broad_rope = rotate(broad_heads[:, :, DB:].astype(jnp.float32), query_pos).astype(jnp.bfloat16)
    narrow_heads = query_narrow.reshape(local_rows, narrow_count, DN + rope_width)
    narrow_nope = narrow_heads[:, :, :DN]
    narrow_rope = rotate(narrow_heads[:, :, DN:].astype(jnp.float32), query_pos).astype(
        jnp.bfloat16
    )
    broad_scale = (DB + rope_width) ** (-0.5)
    narrow_scale = (DN + rope_width) ** (-0.5)

    def attend(running, latent_rows, rope_rows, first_row):
        key_count = latent_rows.shape[0]
        key_pos = first_row + jnp.arange(key_count, dtype=jnp.int32)
        latent_normed = rms_scale(latent_rows.astype(jnp.float32), latent_gain).astype(jnp.bfloat16)

        def expand(weight, head_size):
            product = jnp.dot(latent_normed, weight, preferred_element_type=jnp.float32)
            return product.astype(jnp.bfloat16).reshape(key_count, -1, head_size)

        key_rot = rotate(rope_rows.astype(jnp.float32), key_pos).astype(jnp.bfloat16)
        allowed = (key_pos[None, :] <= query_pos[:, None])[None]
        broad_state = group_update(
            running[0],
            broad_nope,
            broad_rope,
            expand(key_up_broad, DB),
            key_rot,
            expand(value_up_broad, DB),
            broad_scale,
            allowed,
        )
        narrow_state = group_update(
            running[1],
            narrow_nope,
            narrow_rope,
            expand(key_up_narrow, DN),
            key_rot,
            expand(value_up_narrow, DN),
            narrow_scale,
            allowed,
        )
        return (broad_state, narrow_state)

    def fresh(head_count, head_size):
        return (
            jnp.full((head_count, local_rows), masked_score, jnp.float32),
            jnp.zeros((head_count, local_rows), jnp.float32),
            jnp.zeros((local_rows, head_count, head_size), jnp.float32),
        )

    initial = (fresh(broad_count, DB), fresh(narrow_count, DN))
    latent_piece = lax.all_gather(latent, "sp", axis=0, tiled=True)
    rope_piece = lax.all_gather(key_rope, "sp", axis=0, tiled=True)
    piece_rows = latent_piece.shape[0]
    block_rows = math.gcd(piece_rows, 1024)

    def one_block(block_index, carried):
        begin = block_index * block_rows
        latent_block = lax.dynamic_slice_in_dim(latent_piece, begin, block_rows, 0)
        rope_block = lax.dynamic_slice_in_dim(rope_piece, begin, block_rows, 0)

        def unchanged(kept_state):
            return kept_state

        def updated(kept_state):
            return attend(kept_state, latent_block, rope_block, begin)

        return lax.cond(begin > last_query, unchanged, updated, carried)

    final_state = lax.fori_loop(0, piece_rows // block_rows, one_block, initial)

    def finish(running):
        run_max, run_sum, run_acc = running
        return (
            (run_acc / jnp.transpose(run_sum)[:, :, None])
            .astype(jnp.bfloat16)
            .reshape(local_rows, -1)
        )

    attn_broad = finish(final_state[0])
    attn_narrow = finish(final_state[1])
    rows_broad, rows_narrow = (
        lax.all_to_all(attn_broad, "tp", split_axis=0, concat_axis=1, tiled=True),
        lax.all_to_all(attn_narrow, "tp", split_axis=0, concat_axis=1, tiled=True),
    )
    projected = jnp.dot(rows_broad, out_broad, preferred_element_type=jnp.float32) + jnp.dot(
        rows_narrow, out_narrow, preferred_element_type=jnp.float32
    )
    own_resid = lax.dynamic_slice_in_dim(resid, lax.axis_index("tp") * share_rows, share_rows, 0)
    mixed = (own_resid.astype(jnp.float32) + rms_scale(projected, post_gain)).astype(jnp.bfloat16)
    normed = rms_scale(mixed.astype(jnp.float32), ffn_gain).astype(jnp.bfloat16)
    up_full, down_full = (
        lax.all_gather(up_weight, "sp", axis=0, tiled=True),
        lax.all_gather(down_weight, "sp", axis=0, tiled=True),
    )
    hidden = jnp.square(
        jax.nn.relu(
            jnp.dot(
                lax.all_gather(normed, "tp", axis=0, tiled=True),
                up_full,
                preferred_element_type=jnp.float32,
            )
        )
    ).astype(jnp.bfloat16)
    ffn = lax.psum_scatter(
        lax.dot_general(
            hidden, down_full, (((1,), (1,)), ((), ())), preferred_element_type=jnp.float32
        ).astype(jnp.bfloat16),
        "tp",
        scatter_dimension=0,
        tiled=True,
    ).astype(jnp.float32)
    return (mixed.astype(jnp.float32) + rms_scale(ffn, ffn_out_gain)).astype(jnp.bfloat16)

lane_tile = 128
row_parts = 2
mesh_id = pl.DeviceIdType.MESH


def sem_layout(lines, tp, chunks):
    sizes = {
        "lat_z": lines,
        "lat_y": lines,
        "lat_x": 2 * lines,
        "lat_c": 4 * lines,
        "up_z": lines,
        "up_y": lines,
        "up_c": 2 * lines,
        "down_z": 2 * lines,
        "down_y": 2 * lines,
        "down_c": 4 * lines,
        "heads": tp,
        "row_z": lines,
        "row_x": lines,
        "sum_x": chunks * lines,
        "sum_r": chunks * 2,
        "sum_m": chunks,
        "sum_f": chunks,
    }
    base, total = {}, 0
    for name, size in sizes.items():
        base[name] = total
        total += size
    return base, total


def layer_kernel(
    sp,
    tp,
    latent_ref,
    key_rope_ref,
    table_ref,
    latent_gain_ref,
    qb_in,
    qn_in,
    resid_ref,
    kb_ref,
    vb_ref,
    kn_ref,
    vn_ref,
    ob_hbm,
    on_hbm,
    post_ref,
    gain_ref,
    last_ref,
    up_hbm,
    down_hbm,
    out_ref,
    mine_ref,
    qb_ref,
    qn_ref,
    lat,
    top_ref,
    sum_ref,
    acc_ref,
    attn,
    heads,
    ob,
    on,
    up,
    down,
    rows,
    hidden_ref,
    part,
    x_send,
    x_got,
    z_send,
    r_got,
    m_got,
    f_got,
    ffn_ref,
    send_sem,
    recv_sem,
    local_sem,
):
    cols = row_parts
    lines = sp // cols
    chunks = 4
    s = lax.axis_index("sp")
    t = lax.axis_index("tp")
    z = s // cols
    y = s % cols
    core = t % 2
    x = t // 2
    t_core = 2 * x + 1 - core
    t_x = 2 * (1 - x) + core
    t_both = 2 * (1 - x) + 1 - core
    s_y = z * cols + 1 - y
    half = z // 2
    mate = z + 1 - 2 * (z % 2)
    gate = 2 - half
    outer = 3 * (1 - half)
    inner = (z == 1) | (z == 2)
    edge = (z == 0) | (z == 3)
    bf16 = jnp.bfloat16
    f32 = jnp.float32
    share = resid_ref.shape[0] // tp
    block_rows = resid_ref.shape[0]
    width = up.shape[3]
    piece = down.shape[4]
    base, _ = sem_layout(lines, tp, chunks)

    def line(at):
        return (at * cols + y, t)

    peer_y, peer_x, peer_c, peer_b = (s_y, t), (s, t_x), (s, t_core), (s, t_both)
    peers = [line(mate), line(gate), line(outer), peer_y, peer_x, peer_c, peer_b]
    barrier = pltpu.get_barrier_semaphore()
    for peer in peers:
        pl.semaphore_signal(barrier, inc=1, device_id=peer, device_id_type=mesh_id)

    rope = key_rope_ref.shape[1]
    half_rope = rope // 2

    def turn(values, table):
        values = values.astype(f32)
        swapped = jnp.concatenate([values[:, half_rope:], values[:, :half_rope]], axis=1)
        return (values * table[:, :rope] + swapped * table[:, rope:]).astype(bf16)

    latent_width = latent_ref.shape[1]
    mine_rows = pl.ds(pl.multiple_of(t * share, 16), share)
    mine_ref[:, :latent_width] = rms_scale(
        latent_ref[mine_rows, :].astype(f32), latent_gain_ref[...]
    ).astype(bf16)
    mine_ref[:, latent_width:] = turn(key_rope_ref[mine_rows, :], table_ref[mine_rows, :])
    pl.semaphore_wait(barrier, len(peers))

    started = []

    def send(src, dst, peer, recv, cond=None):
        copy = pltpu.make_async_remote_copy(
            src_ref=src,
            dst_ref=dst,
            send_sem=send_sem.at[len(started)],
            recv_sem=recv_sem.at[recv],
            device_id=peer,
            device_id_type=mesh_id,
        )
        started.append((cond, copy))
        if cond is None:
            copy.start()
        else:
            pl.when(cond)(lambda: copy.start())

    def arrive(dst, recv):
        pltpu.make_async_remote_copy(
            src_ref=dst,
            dst_ref=dst,
            send_sem=send_sem.at[0],
            recv_sem=recv_sem.at[recv],
            device_id=peer_c,
            device_id_type=mesh_id,
        ).wait_recv()

    locals_ = []

    def bring(src, dst):
        copy = pltpu.make_async_copy(src, dst, local_sem.at[len(locals_)])
        copy.start()
        locals_.append(copy)
        return copy

    def block(k, flipped):
        return (z - k) * cols + ((1 - y) if flipped else y)

    for k in range(1, lines):
        send(mine_ref, lat.at[s, t], line(z + k), base["lat_z"] + k, z + k < lines)
    send(mine_ref, lat.at[s, t], peer_y, base["lat_y"])
    send(mine_ref, lat.at[s, t], peer_x, base["lat_x"])
    send(mine_ref, lat.at[s, t], peer_c, base["lat_c"])
    own_copy = bring(mine_ref, lat.at[s, t])

    def cut(ref, at, first=0, count=None):
        columns = pl.ds(pl.multiple_of(at * width, width), width)
        return ref.at[pl.ds(first, ref.shape[0] if count is None else count), columns]

    far = (gate, outer, mate)

    def up_at(origin, at):
        return up.at[origin, at]

    def down_at(origin, at, upper):
        return down.at[origin, at // cols, at % cols, upper]

    def send_down(upper):
        for dest in far:
            send(
                cut(down_hbm, dest, upper * piece, piece),
                down_at(core, s, upper),
                line(dest),
                base["down_z"] + upper * lines + z,
            )

    for dest in far:
        send(cut(up_hbm, dest), up_at(core, s), line(dest), base["up_z"] + z)
    own = [bring(cut(up_hbm, z), up_at(core, s))]
    for upper in range(2):
        own.append(
            bring(cut(down_hbm, z, upper * piece, piece), down_at(core, s, upper))
        )
    outs = [bring(ob_hbm, ob), bring(on_hbm, on)]

    for queries, turned, size in ((qb_in, qb_ref, DB), (qn_in, qn_ref, DN)):
        step = size + rope
        for h in range(queries.shape[1] // step):
            middle = h * step + size
            turned[:, h * step : middle] = queries[:, h * step : middle]
            turned[:, middle : middle + rope] = turn(
                queries[:, middle : middle + rope], table_ref[...]
            )

    def when(k):
        return None if k == 0 else z >= k

    def guarded(k, body):
        if k == 0:
            body()
        else:
            pl.when(z >= k)(body)

    def lat_in_z(k):
        held = lat.at[block(k, False), t]
        guarded(k, lambda: arrive(held, base["lat_z"] + k))
        send(held, held, peer_y, base["lat_y"] + k, when(k))
        send(held, held, peer_x, base["lat_x"] + 2 * k, when(k))
        send(held, held, peer_c, base["lat_c"] + 4 * k, when(k))

    def lat_in_y(k):
        held = lat.at[block(k, True), t]
        guarded(k, lambda: arrive(held, base["lat_y"] + k))
        send(held, held, peer_x, base["lat_x"] + 2 * k + 1, when(k))
        send(held, held, peer_c, base["lat_c"] + 4 * k + 1, when(k))

    def lat_in_x(k):
        for i, flipped in enumerate((False, True)):
            held = lat.at[block(k, flipped), t_x]
            guarded(k, lambda: arrive(held, base["lat_x"] + 2 * k + i))
            send(held, held, peer_c, base["lat_c"] + 4 * k + 2 + i, when(k))

    broad = kb_ref.shape[1] // DB
    narrow = kn_ref.shape[1] // DN
    wb = DB + rope
    wn = DN + rope
    keys = cols * block_rows

    def attend(k):
        for i, flipped in enumerate((False, True)):
            arrive(lat.at[block(k, flipped), t_core], base["lat_c"] + 4 * k + i)
            arrive(lat.at[block(k, flipped), t_both], base["lat_c"] + 4 * k + 2 + i)
        both = lat[pl.ds((z - k) * cols, cols)].reshape(keys, latent_width + rope)
        normed = both[:, :latent_width]
        rot = both[:, latent_width:]

        def expand(ref):
            return jnp.dot(normed, ref[...], preferred_element_type=f32).astype(bf16)

        kb, vb, kn, vn = expand(kb_ref), expand(vb_ref), expand(kn_ref), expand(vn_ref)
        if k == 0:
            query_pos = y * block_rows + lax.broadcasted_iota(jnp.int32, (block_rows, keys), 0)
            allowed = lax.broadcasted_iota(jnp.int32, (block_rows, keys), 1) <= query_pos
        for h in range(broad + narrow):
            if h < broad:
                q = qb_ref[:, h * wb : (h + 1) * wb]
                key = jnp.concatenate([kb[:, h * DB : (h + 1) * DB], rot], axis=1)
                v = vb[:, h * DB : (h + 1) * DB]
                scale = wb ** (-0.5)
            else:
                n = h - broad
                q = qn_ref[:, n * wn : (n + 1) * wn]
                key = jnp.concatenate([kn[:, n * DN : (n + 1) * DN], rot], axis=1)
                v = vn
                scale = wn ** (-0.5)
            score = scale * lax.dot_general(
                q, key, (((1,), (1,)), ((), ())), preferred_element_type=f32
            )
            if k == 0:
                score = jnp.where(allowed, score, masked_score)
                new_max = jnp.max(score, axis=-1, keepdims=True)
                e = jnp.where(allowed, jnp.exp(score - new_max), 0.0)
                new_sum = jnp.sum(e, axis=-1, keepdims=True)
                acc_ref[h] = jnp.dot(e.astype(bf16), v, preferred_element_type=f32)
            else:
                old_max = top_ref[h]
                new_max = jnp.maximum(old_max, jnp.max(score, axis=-1, keepdims=True))
                e = jnp.exp(score - new_max)
                factor = jnp.exp(old_max - new_max)
                new_sum = sum_ref[h] * factor + jnp.sum(e, axis=-1, keepdims=True)
                acc_ref[h] = acc_ref[h] * factor + jnp.dot(
                    e.astype(bf16), v, preferred_element_type=f32
                )
            top_ref[h] = new_max
            sum_ref[h] = new_sum

    lat_in_y(0)
    lat_in_x(0)
    lat_in_z(1)
    own_copy.wait()
    attend(0)
    lat_in_y(1)
    lat_in_x(1)
    lat_in_z(2)
    lat_in_z(3)
    guarded(1, lambda: attend(1))
    lat_in_y(2)
    lat_in_y(3)
    send(cut(up_hbm, z), up_at(core, s), peer_y, base["up_y"])
    lat_in_x(2)
    lat_in_x(3)
    send(cut(up_hbm, z), up_at(core, s), peer_c, base["up_c"])
    guarded(2, lambda: attend(2))
    guarded(3, lambda: attend(3))

    parts = [acc_ref[h] / sum_ref[h] for h in range(broad + narrow)]
    for h in range(broad):
        for i in range(tp):
            attn[i, :, h * DB : (h + 1) * DB] = parts[h][i * share : (i + 1) * share].astype(bf16)
    column = lax.broadcasted_iota(jnp.int32, parts[broad].shape, 1)
    merged = parts[broad]
    for n in range(1, narrow):
        merged = jnp.where(column >= n * DN, parts[broad + n], merged)
    for i in range(tp):
        attn[i, :, broad * DB :] = merged[i * share : (i + 1) * share].astype(bf16)

    turned_to = ((t_x, peer_x), (t_both, peer_b), (t_core, peer_c))
    for i, (at, peer) in enumerate(turned_to):
        send(attn.at[at], heads.at[t], peer, base["heads"] + i)
    heads[t] = attn[t]
    for upper in range(2):
        send(
            cut(down_hbm, z, upper * piece, piece),
            down_at(core, s, upper),
            peer_y,
            base["down_y"] + upper * lines,
        )
        send(
            cut(down_hbm, z, upper * piece, piece),
            down_at(core, s, upper),
            peer_c,
            base["down_c"] + upper * 2 * lines,
        )
    for copy in outs:
        copy.wait()
    for i, (at, _) in enumerate(turned_to):
        arrive(heads.at[at], base["heads"] + i)

    broad_width = kb_ref.shape[1]
    narrow_width = kn_ref.shape[1]
    projected = jnp.zeros((share, ob.shape[1]), f32)
    for i in range(tp):
        projected = projected + jnp.dot(
            heads[i, :, :broad_width],
            ob[i * broad_width : (i + 1) * broad_width],
            preferred_element_type=f32,
        )
        projected = projected + jnp.dot(
            heads[i, :, broad_width:],
            on[i * narrow_width : (i + 1) * narrow_width],
            preferred_element_type=f32,
        )
    mixed = (
        resid_ref[pl.ds(pl.multiple_of(t * share, 16), share), :].astype(f32)
        + rms_scale(projected, post_ref[...])
    ).astype(bf16)
    rows[0, z] = rms_scale(mixed.astype(f32), gain_ref[...]).astype(bf16)

    held = rows.at[0, z]
    send(held, held, line(gate), base["row_z"] + z)
    send(held, held, line(mate), base["row_z"] + z)
    send(held, rows.at[1, z], peer_x, base["row_x"])
    send_down(0)

    def up_in_z(i, at):
        held = up_at(core, at * cols + y)
        arrive(held, base["up_z"] + at)
        send(held, held, peer_y, base["up_y"] + 1 + i)
        send(held, held, peer_c, base["up_c"] + 1 + i)

    def up_in_y(i, at):
        held = up_at(core, at * cols + 1 - y)
        arrive(held, base["up_y"] + i)
        send(held, held, peer_c, base["up_c"] + lines + i)

    def row_in(i, at):
        held = rows.at[0, at]
        arrive(held, base["row_z"] + at)
        if i < 2:
            send(held, held, line(mate), base["row_z"] + at, inner)
        send(held, rows.at[1, at], peer_x, base["row_x"] + 1 + i)

    for i, at in enumerate(far):
        up_in_z(i, at)
    row_in(2, mate)
    row_in(0, gate)
    row_in(1, outer)
    send_down(1)
    steps = (z,) + far
    for i, at in enumerate(steps):
        up_in_y(i, at)
    own[0].wait()
    for i, at in enumerate(steps):
        arrive(up_at(1 - core, at * cols + y), base["up_c"] + i)
        arrive(up_at(1 - core, at * cols + 1 - y), base["up_c"] + lines + i)

    deep = sp * up.shape[2]

    def raise_rows(j):
        block_in = rows[j].reshape(lines * share, rows.shape[3])
        for origin in range(2):
            product = jnp.dot(
                block_in, up[origin].reshape(deep, width), preferred_element_type=f32
            )
            hidden_ref[
                j * lines * share : (j + 1) * lines * share, origin * width : (origin + 1) * width
            ] = jnp.square(jnp.maximum(product, 0.0)).astype(bf16)

    raise_rows(0)

    def down_in_z(upper):
        for i, at in enumerate(far):
            held = down_at(core, at * cols + y, upper)
            arrive(held, base["down_z"] + upper * lines + at)
            send(held, held, peer_y, base["down_y"] + upper * lines + 1 + i)
            send(held, held, peer_c, base["down_c"] + upper * 2 * lines + 1 + i)

    def down_in_y(upper):
        for i, at in enumerate(steps):
            held = down_at(core, at * cols + 1 - y, upper)
            arrive(held, base["down_y"] + upper * lines + i)
            send(held, held, peer_c, base["down_c"] + upper * 2 * lines + lines + i)

    units = (gate, outer, mate, z)

    def lower(chunk):
        upper, flipped = chunk // 2, chunk % 2
        column = (1 - y) if flipped else y
        for i, at in enumerate(steps):
            arrive(
                down_at(1 - core, at * cols + column, upper),
                base["down_c"] + upper * 2 * lines + flipped * lines + i,
            )
        total = None
        for origin in range(2):
            weight = down[origin, :, column, upper].reshape(lines * piece, width)
            product = lax.dot_general(
                hidden_ref[:, origin * width : (origin + 1) * width],
                weight,
                (((1,), (1,)), ((), ())),
                preferred_element_type=f32,
            )
            total = product if total is None else total + product
        part[chunk] = total[: lines * share].reshape(part.shape[1:])
        x_send[chunk] = total[lines * share :].astype(bf16).reshape(x_send.shape[1:])
        for i, at in enumerate(units):
            send(
                x_send.at[chunk, at],
                x_got.at[chunk, at],
                peer_x,
                base["sum_x"] + chunk * lines + i,
            )

    def pair(chunk, i):
        at = units[i]
        arrive(x_got.at[chunk, at], base["sum_x"] + chunk * lines + i)
        return part[chunk, at] + x_got[chunk, at].astype(f32)

    def gather_sums(chunk):
        far_sum = [
            pltpu.make_async_remote_copy(
                src_ref=z_send.at[chunk, i],
                dst_ref=r_got.at[chunk, i],
                send_sem=send_sem.at[len(started) + i],
                recv_sem=recv_sem.at[base["sum_r"] + chunk * 2 + i],
                device_id=line(mate),
                device_id_type=mesh_id,
            )
            for i in range(2)
        ]
        started.extend((edge, copy) for copy in far_sum)
        mate_sum = pltpu.make_async_remote_copy(
            src_ref=z_send.at[chunk, 2],
            dst_ref=m_got.at[chunk],
            send_sem=send_sem.at[len(started)],
            recv_sem=recv_sem.at[base["sum_m"] + chunk],
            device_id=line(mate),
            device_id_type=mesh_id,
        )
        started.append((None, mate_sum))
        across = [
            pltpu.make_async_remote_copy(
                src_ref=z_send.at[chunk, i],
                dst_ref=f_got.at[chunk],
                send_sem=send_sem.at[len(started) + i],
                recv_sem=recv_sem.at[base["sum_f"] + chunk],
                device_id=line(units[i]),
                device_id_type=mesh_id,
            )
            for i in range(2)
        ]
        started.extend((inner, copy) for copy in across)

        @pl.when(edge)
        def _():
            for i in range(2):
                z_send[chunk, i] = pair(chunk, i).astype(bf16)
                far_sum[i].start()
            z_send[chunk, 2] = pair(chunk, 2).astype(bf16)
            mate_sum.start()

        @pl.when(inner)
        def _():
            z_send[chunk, 2] = pair(chunk, 2).astype(bf16)
            mate_sum.start()
            for i in range(2):
                value = pair(chunk, i)
                arrive(r_got.at[chunk, i], base["sum_r"] + chunk * 2 + i)
                z_send[chunk, i] = (value + r_got[chunk, i].astype(f32)).astype(bf16)
                across[i].start()

    def finish(chunk):
        upper, flipped = chunk // 2, chunk % 2
        column = (1 - y) if flipped else y
        value = pair(chunk, 3)
        arrive(m_got.at[chunk], base["sum_m"] + chunk)
        value = value + m_got[chunk].astype(f32)
        arrive(f_got.at[chunk], base["sum_f"] + chunk)
        value = value + f_got[chunk].astype(f32)
        for i in range(lines):
            start = pl.multiple_of(((i * cols + column) * 2 + upper) * piece, piece)
            ffn_ref[:, pl.ds(start, piece)] = value[:, i * piece : (i + 1) * piece]

    down_in_z(0)
    for i, at in enumerate((z, gate, outer, mate)):
        arrive(rows.at[1, at], base["row_x"] + i)
    raise_rows(1)
    own[1].wait()
    own[2].wait()
    lower(0)
    down_in_y(0)
    lower(1)
    gather_sums(0)
    down_in_z(1)
    lower(2)
    gather_sums(1)
    down_in_y(1)
    lower(3)
    gather_sums(2)
    finish(0)
    finish(1)
    gather_sums(3)
    finish(2)
    finish(3)
    out_ref[...] = (mixed.astype(f32) + rms_scale(ffn_ref[...], last_ref[...])).astype(bf16)
    for cond, copy in started:
        if cond is None:
            copy.wait_send()
        else:
            pl.when(cond)(lambda: copy.wait_send())


def fast_local(
    resid,
    query_broad,
    query_narrow,
    latent,
    key_rope,
    latent_gain,
    key_up_broad,
    value_up_broad,
    key_up_narrow,
    value_up_narrow,
    out_broad,
    out_narrow,
    post_gain,
    ffn_gain,
    up_weight,
    down_weight,
    ffn_out_gain,
):
    sp = lax.axis_size("sp")
    tp = lax.axis_size("tp")
    cols = row_parts
    lines = sp // cols
    s = lax.axis_index("sp")
    z = s // cols
    y = s % cols
    local_rows = resid.shape[0]
    share_rows = local_rows // tp
    query_pos = s * local_rows + jnp.arange(local_rows, dtype=jnp.int32)
    rope_width = key_rope.shape[1]
    bf16 = jnp.bfloat16

    frequency = rope_base ** (-2.0 * jnp.arange(rope_width // 2, dtype=jnp.float32) / rope_width)
    angles = query_pos.astype(jnp.float32)[:, None] * frequency[None, :]
    cosine, sine = jnp.cos(angles), jnp.sin(angles)
    table = jnp.concatenate([cosine, cosine, -sine, sine], axis=1)
    half_rows = local_rows // 2
    both_width = latent.shape[1] + rope_width
    broad_width = key_up_broad.shape[1]
    narrow_width = key_up_narrow.shape[1]
    width = broad_width + narrow_width
    deep = resid.shape[1]
    slice_width = up_weight.shape[1] // lines
    vmem = pl.BlockSpec(memory_space=pltpu.VMEM)
    anywhere = pl.BlockSpec(memory_space=pl.ANY)
    chunks = 4
    heads = broad_width // DB + narrow_width // DN
    piece = up_weight.shape[0] // 2
    chunk_width = deep // chunks
    _, sems = sem_layout(lines, tp, chunks)
    f32 = jnp.float32
    return pl.pallas_call(
        functools.partial(layer_kernel, sp, tp),
        out_shape=jax.ShapeDtypeStruct((share_rows, deep), bf16),
        in_specs=[vmem] * 11 + [anywhere] * 2 + [vmem] * 3 + [anywhere] * 2,
        out_specs=vmem,
        scratch_shapes=[
            pltpu.VMEM((share_rows, both_width), bf16),
            pltpu.VMEM(query_broad.shape, bf16),
            pltpu.VMEM(query_narrow.shape, bf16),
            pltpu.VMEM((sp, tp, share_rows, both_width), bf16),
            pltpu.VMEM((heads, local_rows, 1), f32),
            pltpu.VMEM((heads, local_rows, 1), f32),
            pltpu.VMEM((heads, local_rows, lane_tile), f32),
            pltpu.VMEM((tp, share_rows, width), bf16),
            pltpu.VMEM((tp, share_rows, width), bf16),
            pltpu.VMEM(out_broad.shape, bf16),
            pltpu.VMEM(out_narrow.shape, bf16),
            pltpu.VMEM((2, sp, up_weight.shape[0], slice_width), bf16),
            pltpu.VMEM((2, lines, cols, 2, piece, slice_width), bf16),
            pltpu.VMEM((2, lines, share_rows, deep), bf16),
            pltpu.VMEM((2 * lines * share_rows, 2 * slice_width), bf16),
            pltpu.VMEM((chunks, lines, share_rows, chunk_width), f32),
            pltpu.VMEM((chunks, lines, share_rows, chunk_width), bf16),
            pltpu.VMEM((chunks, lines, share_rows, chunk_width), bf16),
            pltpu.VMEM((chunks, 3, share_rows, chunk_width), bf16),
            pltpu.VMEM((chunks, 2, share_rows, chunk_width), bf16),
            pltpu.VMEM((chunks, share_rows, chunk_width), bf16),
            pltpu.VMEM((chunks, share_rows, chunk_width), bf16),
            pltpu.VMEM((share_rows, deep), f32),
            pltpu.SemaphoreType.DMA((sems + lines * tp,)),
            pltpu.SemaphoreType.DMA((sems,)),
            pltpu.SemaphoreType.DMA((6,)),
        ],
        compiler_params=pltpu.CompilerParams(
            collective_id=0, has_side_effects=True, vmem_limit_bytes=60 * 2**20
        ),
    )(
        latent,
        key_rope,
        table,
        latent_gain[None],
        query_broad,
        query_narrow,
        resid,
        key_up_broad,
        value_up_broad,
        key_up_narrow,
        value_up_narrow,
        out_broad,
        out_narrow,
        post_gain[None],
        ffn_gain[None],
        ffn_out_gain[None],
        up_weight,
        down_weight,
    )


def solution(mesh):
    in_specs = (
        P("sp", None),
        P("sp", "tp"),
        P("sp", "tp"),
        P("sp", None),
        P("sp", None),
        P(),
        P(None, "tp"),
        P(None, "tp"),
        P(None, "tp"),
        P(None, "tp"),
        P(),
        P(),
        P(),
        P(),
        P("sp", "tp"),
        P("sp", "tp"),
        P(),
    )
    out_specs = P(("sp", "tp"), None)
    sp = mesh.shape["sp"]
    tp = mesh.shape["tp"]

    def whole(*args):
        hidden = args[14].shape[1] // tp
        rows = args[0].shape[0] // sp
        lines = sp // row_parts
        fits = (
            sp % row_parts == 0
            and tp & (tp - 1) == 0
            and tp == 4
            and lines == 4
            and hidden % (lines * lane_tile) == 0
            and args[0].shape[1] % (2 * lane_tile * sp) == 0
            and rows % (16 * tp) == 0
        )
        body = fast_local if fits else local
        return jax.shard_map(
            body, mesh=mesh, in_specs=in_specs, out_specs=out_specs, check_vma=False
        )(*args)

    return whole
```

time: 123 us -> 118 us (0.959)
  Pallas kernels: 118 us -> 113 us
    pallas_call x1, Pallas kernels: 118 us -> 113 us  [fast_local(): pl.pallas_call(functools.partial(layer_kernel, sp, tp), out_shape=jax.Sha...]
where the time goes in v1:
time: 118 us
  Pallas kernels  113 us (96%)
  local copies, waits for them, and re-layouts  3.09 us (3%)
  other arithmetic  1.23 us (1%)
    pallas_call x1, Pallas kernels, fast_local(): pl.pallas_call(functools.partial(layer_kernel, sp, tp), out_shape=jax.Sha...  113 us
    unnamed x2, local copies, waits for them, and re-layouts  3.09 us

profile of v1, /device:TPU:0, one launch (start us, length us, event | category | flops | bytes accessed | tf_op | source)
XLA Modules:
  0.0 117.5 jit_solution(18200906504227503070)
XLA Ops:
  0.0 0.4 multiply_cosine_fusion
  0.4 0.8 pad_maximum_fusion.table_ref
  1.2 1.5 %copy.20.key_rope_ref = bf16[192,64]{1,0:T(8,128)(2,1)} copy(bf16[192,64]{0,1:T(8,128)(2,1)} %param.21) | data formatting | bytes 49152 | tf_op args[4]
  2.7 113.2 %shard_map.163 = bf16[48,2048]{1,0:T(8,128)(2,1)} custom-call(bf16[192,512]{1,0:T(8,128)(2,1)} %latent_ref.1, bf16[192,64]{1,0:T(8,128)(2,1)} %copy.20.key_rope_ref, f32[192,128]{1,0:T(8,128)} %pad_maximum_fusion.table_ref, f32[1,512]{1,0:T(1,128)} %bitcast.7, bf16[192,384]{1,0:T(8,128)(2,1)} %qb_in.1, bf16[192,256]{1,0:T(8,128)(2,1)} %qn_in.1, ...), custom_call_target="tpu_custom_call" | custom-call | tf_op jit(solution)/shard_map/pallas_call | solution.py:823
  115.9 1.6 %copy.22 = bf16[48,2048]{1,0:T(8,128)(2,1)} copy(bf16[48,2048]{1,0:T(8,128)(2,1)} %shard_map.163) | data formatting | bytes 393216
  (2 shorter events, 0.0 us)

commit v2 on v1

--- a/solution.py
+++ b/solution.py
@@ -209,7 +209,7 @@
 mesh_id = pl.DeviceIdType.MESH
 
 
-def sem_layout(lines, tp, chunks):
+def sem_layout(lines, tp, chunks, row_chunks):
     sizes = {
         "lat_z": lines,
         "lat_y": lines,
@@ -222,8 +222,8 @@
         "down_y": 2 * lines,
         "down_c": 4 * lines,
         "heads": tp,
-        "row_z": lines,
-        "row_x": lines,
+        "row_z": lines * row_chunks,
+        "row_x": lines * row_chunks,
         "sum_x": chunks * lines,
         "sum_r": chunks * 2,
         "sum_m": chunks,
@@ -284,10 +284,12 @@
     send_sem,
     recv_sem,
     local_sem,
+    pair_sem,
 ):
     cols = row_parts
     lines = sp // cols
-    chunks = 4
+    groups = ((1, 2), (0, 3))
+    chunks = len(groups)
     s = lax.axis_index("sp")
     t = lax.axis_index("tp")
     z = s // cols
@@ -309,8 +311,9 @@
     share = resid_ref.shape[0] // tp
     block_rows = resid_ref.shape[0]
     width = up.shape[3]
-    piece = down.shape[4]
-    base, _ = sem_layout(lines, tp, chunks)
+    row_step = 16
+    row_chunks = share // row_step
+    base, _ = sem_layout(lines, tp, chunks, row_chunks)
 
     def line(at):
         return (at * cols + y, t)
@@ -375,41 +378,48 @@
     def block(k, flipped):
         return (z - k) * cols + ((1 - y) if flipped else y)
 
-    for k in range(1, lines):
+    for k in range(lines - 1, 0, -1):
         send(mine_ref, lat.at[s, t], line(z + k), base["lat_z"] + k, z + k < lines)
     send(mine_ref, lat.at[s, t], peer_y, base["lat_y"])
     send(mine_ref, lat.at[s, t], peer_x, base["lat_x"])
     send(mine_ref, lat.at[s, t], peer_c, base["lat_c"])
     own_copy = bring(mine_ref, lat.at[s, t])
 
-    def cut(ref, at, first=0, count=None):
-        columns = pl.ds(pl.multiple_of(at * width, width), width)
-        return ref.at[pl.ds(first, ref.shape[0] if count is None else count), columns]
+    def cut(ref, at):
+        return ref.at[:, pl.ds(pl.multiple_of(at * width, width), width)]
 
     far = (gate, outer, mate)
 
     def up_at(origin, at):
         return up.at[origin, at]
 
-    def down_at(origin, at, upper):
-        return down.at[origin, at // cols, at % cols, upper]
-
-    def send_down(upper):
-        for dest in far:
+    def down_at(origin, at, flipped=False):
+        return down.at[origin, at, (1 - y) if flipped else y]
+
+    def send_down(dest, cond=None):
+        for i in range(2):
             send(
-                cut(down_hbm, dest, upper * piece, piece),
-                down_at(core, s, upper),
+                down_half(cut(down_hbm, dest), i),
+                down_half(down_at(core, z), i),
                 line(dest),
-                base["down_z"] + upper * lines + z,
+                base["down_z"] + 2 * z + i,
+                cond,
             )
 
+    def down_half(ref, i):
+        rows_half = down.shape[3] // 2
+        return ref.at[pl.ds(i * rows_half, rows_half)]
+
+    def send_up(dest, cond):
+        send(cut(up_hbm, dest), up_at(core, s), line(dest), base["up_z"] + z, cond)
+
+    send_up(mate, edge)
     for dest in far:
-        send(cut(up_hbm, dest), up_at(core, s), line(dest), base["up_z"] + z)
+        send_up(dest, None if dest is not mate else inner)
+    send_down(mate, inner)
+    send_down(gate, z == 2)
     own = [bring(cut(up_hbm, z), up_at(core, s))]
-    for upper in range(2):
-        own.append(
-            bring(cut(down_hbm, z, upper * piece, piece), down_at(core, s, upper))
-        )
+    own.append(bring(cut(down_hbm, z), down_at(core, z)))
     outs = [bring(ob_hbm, ob), bring(on_hbm, on)]
 
     for queries, turned, size in ((qb_in, qb_ref, DB), (qn_in, qn_ref, DN)):
@@ -503,22 +513,44 @@
             top_ref[h] = new_max
             sum_ref[h] = new_sum
 
+    def up_in_z(i, at):
+        held = up_at(core, at * cols + y)
+        arrive(held, base["up_z"] + at)
+        send(held, held, peer_y, base["up_y"] + 1 + i)
+        send(held, held, peer_c, base["up_c"] + 1 + i)
+
+    def down_in_z(at, cond=None):
+        for i in range(2):
+            held = down_half(down_at(core, at), i)
+            if cond is None:
+                arrive(held, base["down_z"] + 2 * at + i)
+            else:
+                pl.when(cond)(lambda: arrive(held, base["down_z"] + 2 * at + i))
+            send(held, held, peer_y, base["down_y"] + 2 * at + i, cond)
+            send(held, held, peer_c, base["down_c"] + 4 * at + i, cond)
+
     lat_in_y(0)
+    lat_in_z(1)
+    lat_in_z(2)
+    lat_in_z(3)
     lat_in_x(0)
-    lat_in_z(1)
+    send(cut(up_hbm, z), up_at(core, s), peer_y, base["up_y"])
+    send(cut(up_hbm, z), up_at(core, s), peer_c, base["up_c"])
     own_copy.wait()
     attend(0)
     lat_in_y(1)
-    lat_in_x(1)
-    lat_in_z(2)
-    lat_in_z(3)
-    guarded(1, lambda: attend(1))
     lat_in_y(2)
     lat_in_y(3)
-    send(cut(up_hbm, z), up_at(core, s), peer_y, base["up_y"])
+    lat_in_x(1)
+    up_in_z(2, mate)
+    for i in range(2):
+        held = down_half(cut(down_hbm, z), i)
+        own_half = down_half(down_at(core, z), i)
+        send(held, own_half, peer_y, base["down_y"] + 2 * z + i)
+        send(held, own_half, peer_c, base["down_c"] + 4 * z + i)
+    guarded(1, lambda: attend(1))
     lat_in_x(2)
     lat_in_x(3)
-    send(cut(up_hbm, z), up_at(core, s), peer_c, base["up_c"])
     guarded(2, lambda: attend(2))
     guarded(3, lambda: attend(3))
 
@@ -537,24 +569,12 @@
     for i, (at, peer) in enumerate(turned_to):
         send(attn.at[at], heads.at[t], peer, base["heads"] + i)
     heads[t] = attn[t]
-    for upper in range(2):
-        send(
-            cut(down_hbm, z, upper * piece, piece),
-            down_at(core, s, upper),
-            peer_y,
-            base["down_y"] + upper * lines,
-        )
-        send(
-            cut(down_hbm, z, upper * piece, piece),
-            down_at(core, s, upper),
-            peer_c,
-            base["down_c"] + upper * 2 * lines,
-        )
     for copy in outs:
         copy.wait()
     for i, (at, _) in enumerate(turned_to):
         arrive(heads.at[at], base["heads"] + i)
 
+    down_in_z(mate, edge)
     broad_width = kb_ref.shape[1]
     narrow_width = kn_ref.shape[1]
     projected = jnp.zeros((share, ob.shape[1]), f32)
@@ -575,17 +595,20 @@
     ).astype(bf16)
     rows[0, z] = rms_scale(mixed.astype(f32), gain_ref[...]).astype(bf16)
 
-    held = rows.at[0, z]
-    send(held, held, line(gate), base["row_z"] + z)
-    send(held, held, line(mate), base["row_z"] + z)
-    send(held, rows.at[1, z], peer_x, base["row_x"])
-    send_down(0)
-
-    def up_in_z(i, at):
-        held = up_at(core, at * cols + y)
-        arrive(held, base["up_z"] + at)
-        send(held, held, peer_y, base["up_y"] + 1 + i)
-        send(held, held, peer_c, base["up_c"] + 1 + i)
+    def row_piece(side, at, c):
+        return rows.at[side, at, pl.ds(c * row_step, row_step)]
+
+    crossing = []
+    for dest in (gate, mate):
+        for c in range(row_chunks):
+            held = row_piece(0, z, c)
+            send(held, held, line(dest), base["row_z"] + z * row_chunks + c)
+            if dest is gate:
+                crossing.append(started.pop()[1])
+                started.append((edge, crossing[-1]))
+                send(held, row_piece(1, z, c), peer_x, base["row_x"] + c)
+    send_down(mate, edge)
+    send_down(gate, z == 3)
 
     def up_in_y(i, at):
         held = up_at(core, at * cols + 1 - y)
@@ -593,19 +616,30 @@
         send(held, held, peer_c, base["up_c"] + lines + i)
 
     def row_in(i, at):
-        held = rows.at[0, at]
-        arrive(held, base["row_z"] + at)
-        if i < 2:
-            send(held, held, line(mate), base["row_z"] + at, inner)
-        send(held, rows.at[1, at], peer_x, base["row_x"] + 1 + i)
-
-    for i, at in enumerate(far):
-        up_in_z(i, at)
+        for c in range(row_chunks):
+            held = row_piece(0, at, c)
+            index = base["row_z"] + at * row_chunks + c
+            arrive(held, index)
+            if i < 2:
+                send(held, held, line(mate), index, inner)
+            send(held, row_piece(1, at, c), peer_x, base["row_x"] + (1 + i) * row_chunks + c)
+
+    up_in_z(0, gate)
+    up_in_z(1, outer)
     row_in(2, mate)
     row_in(0, gate)
     row_in(1, outer)
-    send_down(1)
+    @pl.when(inner)
+    def _():
+        for copy in crossing:
+            copy.wait_send()
+        pl.semaphore_signal(pair_sem, inc=1, device_id=peer_c, device_id_type=mesh_id)
+        pl.semaphore_wait(pair_sem, 1)
+
+    send_down(gate, z == 1)
+    send_down(outer, inner)
     steps = (z,) + far
+    down_in_z(mate, inner)
     for i, at in enumerate(steps):
         up_in_y(i, at)
     own[0].wait()
@@ -626,48 +660,43 @@
             ] = jnp.square(jnp.maximum(product, 0.0)).astype(bf16)
 
     raise_rows(0)
-
-    def down_in_z(upper):
-        for i, at in enumerate(far):
-            held = down_at(core, at * cols + y, upper)
-            arrive(held, base["down_z"] + upper * lines + at)
-            send(held, held, peer_y, base["down_y"] + upper * lines + 1 + i)
-            send(held, held, peer_c, base["down_c"] + upper * 2 * lines + 1 + i)
-
-    def down_in_y(upper):
-        for i, at in enumerate(steps):
-            held = down_at(core, at * cols + 1 - y, upper)
-            arrive(held, base["down_y"] + upper * lines + i)
-            send(held, held, peer_c, base["down_c"] + upper * 2 * lines + lines + i)
+    send_down(gate, z == 0)
+    send_down(outer, edge)
+
+    def down_in_y(at):
+        for i in range(2):
+            held = down_half(down_at(core, at, True), i)
+            arrive(held, base["down_y"] + 2 * at + i)
+            send(held, held, peer_c, base["down_c"] + 4 * at + 2 + i)
 
     units = (gate, outer, mate, z)
 
-    def lower(chunk):
-        upper, flipped = chunk // 2, chunk % 2
-        column = (1 - y) if flipped else y
-        for i, at in enumerate(steps):
-            arrive(
-                down_at(1 - core, at * cols + column, upper),
-                base["down_c"] + upper * 2 * lines + flipped * lines + i,
-            )
-        total = None
-        for origin in range(2):
-            weight = down[origin, :, column, upper].reshape(lines * piece, width)
-            product = lax.dot_general(
-                hidden_ref[:, origin * width : (origin + 1) * width],
-                weight,
-                (((1,), (1,)), ((), ())),
-                preferred_element_type=f32,
-            )
-            total = product if total is None else total + product
-        part[chunk] = total[: lines * share].reshape(part.shape[1:])
-        x_send[chunk] = total[lines * share :].astype(bf16).reshape(x_send.shape[1:])
+    span = part.shape[3] // 2
+
+    def lower(group):
+        for j, at in enumerate(groups[group]):
+            for k, flipped in enumerate((False, True)):
+                for i in range(2):
+                    held = down_half(down_at(1 - core, at, flipped), i)
+                    arrive(held, base["down_c"] + 4 * at + 2 * k + i)
+            total = None
+            for origin in range(2):
+                product = lax.dot_general(
+                    hidden_ref[:, origin * width : (origin + 1) * width],
+                    down[origin, at].reshape(span, width),
+                    (((1,), (1,)), ((), ())),
+                    preferred_element_type=f32,
+                )
+                total = product if total is None else total + product
+            total = total.reshape(2, lines, share, span)
+            part[group, :, :, j * span : (j + 1) * span] = total[0]
+            x_send[group, :, :, j * span : (j + 1) * span] = total[1].astype(bf16)
         for i, at in enumerate(units):
             send(
-                x_send.at[chunk, at],
-                x_got.at[chunk, at],
+                x_send.at[group, at],
+                x_got.at[group, at],
                 peer_x,
-                base["sum_x"] + chunk * lines + i,
+                base["sum_x"] + group * lines + i,
             )
 
     def pair(chunk, i):
@@ -710,16 +739,14 @@
         ]
         started.extend((inner, copy) for copy in across)
 
-        @pl.when(edge)
-        def _():
+        def edge_part():
             for i in range(2):
                 z_send[chunk, i] = pair(chunk, i).astype(bf16)
                 far_sum[i].start()
             z_send[chunk, 2] = pair(chunk, 2).astype(bf16)
             mate_sum.start()
 
-        @pl.when(inner)
-        def _():
+        def inner_part():
             z_send[chunk, 2] = pair(chunk, 2).astype(bf16)
             mate_sum.start()
             for i in range(2):
@@ -728,39 +755,35 @@
                 z_send[chunk, i] = (value + r_got[chunk, i].astype(f32)).astype(bf16)
                 across[i].start()
 
+        pl.when(edge)(edge_part)
+        pl.when(inner)(inner_part)
+
     def finish(chunk):
-        upper, flipped = chunk // 2, chunk % 2
-        column = (1 - y) if flipped else y
         value = pair(chunk, 3)
         arrive(m_got.at[chunk], base["sum_m"] + chunk)
         value = value + m_got[chunk].astype(f32)
         arrive(f_got.at[chunk], base["sum_f"] + chunk)
         value = value + f_got[chunk].astype(f32)
-        for i in range(lines):
-            start = pl.multiple_of(((i * cols + column) * 2 + upper) * piece, piece)
-            ffn_ref[:, pl.ds(start, piece)] = value[:, i * piece : (i + 1) * piece]
-
-    down_in_z(0)
+        for j, at in enumerate(groups[chunk]):
+            ffn_ref[:, at * span : (at + 1) * span] = value[:, j * span : (j + 1) * span]
+
     for i, at in enumerate((z, gate, outer, mate)):
-        arrive(rows.at[1, at], base["row_x"] + i)
+        for c in range(row_chunks):
+            arrive(row_piece(1, at, c), base["row_x"] + i * row_chunks + c)
     raise_rows(1)
     own[1].wait()
-    own[2].wait()
+    down_in_z(gate)
+    down_in_y(1)
+    down_in_y(2)
     lower(0)
+    down_in_z(outer)
     down_in_y(0)
+    down_in_y(3)
     lower(1)
     gather_sums(0)
-    down_in_z(1)
-    lower(2)
     gather_sums(1)
-    down_in_y(1)
-    lower(3)
-    gather_sums(2)
     finish(0)
     finish(1)
-    gather_sums(3)
-    finish(2)
-    finish(3)
     out_ref[...] = (mixed.astype(f32) + rms_scale(ffn_ref[...], last_ref[...])).astype(bf16)
     for cond, copy in started:
         if cond is None:
@@ -814,11 +837,10 @@
     slice_width = up_weight.shape[1] // lines
     vmem = pl.BlockSpec(memory_space=pltpu.VMEM)
     anywhere = pl.BlockSpec(memory_space=pl.ANY)
-    chunks = 4
+    chunks = 2
     heads = broad_width // DB + narrow_width // DN
-    piece = up_weight.shape[0] // 2
     chunk_width = deep // chunks
-    _, sems = sem_layout(lines, tp, chunks)
+    _, sems = sem_layout(lines, tp, chunks, share_rows // 16)
     f32 = jnp.float32
     return pl.pallas_call(
         functools.partial(layer_kernel, sp, tp),
@@ -838,7 +860,7 @@
             pltpu.VMEM(out_broad.shape, bf16),
             pltpu.VMEM(out_narrow.shape, bf16),
             pltpu.VMEM((2, sp, up_weight.shape[0], slice_width), bf16),
-            pltpu.VMEM((2, lines, cols, 2, piece, slice_width), bf16),
+            pltpu.VMEM((2, lines, cols, down_weight.shape[0], slice_width), bf16),
             pltpu.VMEM((2, lines, share_rows, deep), bf16),
             pltpu.VMEM((2 * lines * share_rows, 2 * slice_width), bf16),
             pltpu.VMEM((chunks, lines, share_rows, chunk_width), f32),
@@ -849,9 +871,10 @@
             pltpu.VMEM((chunks, share_rows, chunk_width), bf16),
             pltpu.VMEM((chunks, share_rows, chunk_width), bf16),
             pltpu.VMEM((share_rows, deep), f32),
-            pltpu.SemaphoreType.DMA((sems + lines * tp,)),
+            pltpu.SemaphoreType.DMA((2 * sems,)),
             pltpu.SemaphoreType.DMA((sems,)),
-            pltpu.SemaphoreType.DMA((6,)),
+            pltpu.SemaphoreType.DMA((5,)),
+            pltpu.SemaphoreType.REGULAR,
         ],
         compiler_params=pltpu.CompilerParams(
             collective_id=0, has_side_effects=True, vmem_limit_bytes=60 * 2**20

time: 118 us -> 110 us (0.932)
  Pallas kernels: 113 us -> 105 us
    pallas_call x1, Pallas kernels: 113 us -> 105 us  [fast_local(): pl.pallas_call(functools.partial(layer_kernel, sp, tp), out_shape=jax.Sha...]
where the time goes in v2:
time: 110 us; the launch traced here: 109 us
  Pallas kernels  105 us (95%)
  local copies, waits for them, and re-layouts  3.09 us (3%)
  other arithmetic  1.23 us (1%)
    pallas_call x1, Pallas kernels, fast_local(): pl.pallas_call(functools.partial(layer_kernel, sp, tp), out_shape=jax.Sha...  105 us
    unnamed x2, local copies, waits for them, and re-layouts  3.09 us

profile of v2, /device:TPU:0, one launch (start us, length us, event | category | flops | bytes accessed | tf_op | source)
XLA Modules:
  0.0 109.5 jit_solution(18108357657872267444)
XLA Ops:
  0.0 0.4 multiply_cosine_fusion
  0.4 0.8 pad_maximum_fusion.table_ref
  1.2 1.5 %copy.20.key_rope_ref = bf16[192,64]{1,0:T(8,128)(2,1)} copy(bf16[192,64]{0,1:T(8,128)(2,1)} %param.21) | data formatting | bytes 49152 | tf_op args[4]
  2.7 105.1 %shard_map.163 = bf16[48,2048]{1,0:T(8,128)(2,1)} custom-call(bf16[192,512]{1,0:T(8,128)(2,1)} %latent_ref.1, bf16[192,64]{1,0:T(8,128)(2,1)} %copy.20.key_rope_ref, f32[192,128]{1,0:T(8,128)} %pad_maximum_fusion.table_ref, f32[1,512]{1,0:T(1,128)} %bitcast.7, bf16[192,384]{1,0:T(8,128)(2,1)} %qb_in.1, bf16[192,256]{1,0:T(8,128)(2,1)} %qn_in.1, ...), custom_call_target="tpu_custom_call" | custom-call | tf_op jit(solution)/shard_map/pallas_call | solution.py:845
  107.9 1.6 %copy.22 = bf16[48,2048]{1,0:T(8,128)(2,1)} copy(bf16[48,2048]{1,0:T(8,128)(2,1)} %shard_map.163) | data formatting | bytes 393216
  (2 shorter events, 0.0 us)

commit v3 on v2

--- a/solution.py
+++ b/solution.py
@@ -288,8 +288,7 @@
 ):
     cols = row_parts
     lines = sp // cols
-    groups = ((1, 2), (0, 3))
-    chunks = len(groups)
+    chunks = 5
     s = lax.axis_index("sp")
     t = lax.axis_index("tp")
     z = s // cols
@@ -640,6 +639,7 @@
     send_down(outer, inner)
     steps = (z,) + far
     down_in_z(mate, inner)
+    down_in_z(gate, edge)
     for i, at in enumerate(steps):
         up_in_y(i, at)
     own[0].wait()
@@ -671,119 +671,153 @@
 
     units = (gate, outer, mate, z)
 
-    span = part.shape[3] // 2
-
-    def lower(group):
-        for j, at in enumerate(groups[group]):
-            for k, flipped in enumerate((False, True)):
-                for i in range(2):
-                    held = down_half(down_at(1 - core, at, flipped), i)
-                    arrive(held, base["down_c"] + 4 * at + 2 * k + i)
-            total = None
-            for origin in range(2):
-                product = lax.dot_general(
-                    hidden_ref[:, origin * width : (origin + 1) * width],
-                    down[origin, at].reshape(span, width),
-                    (((1,), (1,)), ((), ())),
-                    preferred_element_type=f32,
-                )
-                total = product if total is None else total + product
-            total = total.reshape(2, lines, share, span)
-            part[group, :, :, j * span : (j + 1) * span] = total[0]
-            x_send[group, :, :, j * span : (j + 1) * span] = total[1].astype(bf16)
+    deep_part = down.shape[3]
+    early = (lines - 1) * half
+    late = (lines - 1) * (1 - half)
+
+    def sibling_in(at, flipped):
+        for i in range(2):
+            held = down_half(down_at(1 - core, at, flipped), i)
+            arrive(held, base["down_c"] + 4 * at + 2 * flipped + i)
+
+    def columns_of(start, count):
+        if not isinstance(start, int):
+            start = pl.multiple_of(start, lane_tile)
+        return pl.ds(start, count)
+
+    def lower(weights, columns):
+        total = None
+        for origin in range(2):
+            product = lax.dot_general(
+                hidden_ref[:, origin * width : (origin + 1) * width],
+                weights(origin),
+                (((1,), (1,)), ((), ())),
+                preferred_element_type=f32,
+            )
+            total = product if total is None else total + product
+        total = total.reshape(2, lines, share, total.shape[1])
+        part[:, :, columns] = total[0]
+        x_send[:, :, columns] = total[1].astype(bf16)
+
+    def send_sums(group, columns):
         for i, at in enumerate(units):
             send(
-                x_send.at[group, at],
-                x_got.at[group, at],
+                x_send.at[at, :, columns],
+                x_got.at[at, :, columns],
                 peer_x,
                 base["sum_x"] + group * lines + i,
             )
 
-    def pair(chunk, i):
+    def lower_middle():
+        for at in (1, 2):
+            sibling_in(at, 0)
+            sibling_in(at, 1)
+        wide = 2 * cols * deep_part
+        columns = pl.ds(cols * deep_part, wide)
+        lower(lambda origin: down[origin, 1:3].reshape(wide, width), columns)
+        send_sums(0, columns)
+        return 0, columns
+
+    def lower_edge(at, flipped):
+        sibling_in(at, flipped)
+        side = (1 - y) if flipped else y
+        columns = columns_of((at * cols + side) * deep_part, deep_part)
+        lower(lambda origin: down[origin, at, side], columns)
+        group = 1 + 2 * (at // (lines - 1)) + flipped
+        send_sums(group, columns)
+        return group, columns
+
+    def pair(group, columns, i):
         at = units[i]
-        arrive(x_got.at[chunk, at], base["sum_x"] + chunk * lines + i)
-        return part[chunk, at] + x_got[chunk, at].astype(f32)
-
-    def gather_sums(chunk):
-        far_sum = [
-            pltpu.make_async_remote_copy(
-                src_ref=z_send.at[chunk, i],
-                dst_ref=r_got.at[chunk, i],
-                send_sem=send_sem.at[len(started) + i],
-                recv_sem=recv_sem.at[base["sum_r"] + chunk * 2 + i],
-                device_id=line(mate),
-                device_id_type=mesh_id,
+        arrive(x_got.at[at, :, columns], base["sum_x"] + group * lines + i)
+        return part[at, :, columns] + x_got[at, :, columns].astype(f32)
+
+    def sum_copy(i, got, peer, index, cond, columns):
+        copy = pltpu.make_async_remote_copy(
+            src_ref=z_send.at[i, :, columns],
+            dst_ref=got.at[:, columns],
+            send_sem=send_sem.at[len(started)],
+            recv_sem=recv_sem.at[index],
+            device_id=peer,
+            device_id_type=mesh_id,
+        )
+        started.append((cond, copy))
+        return copy
+
+    def combine(group, columns):
+        near = [
+            sum_copy(
+                i, r_got.at[i], line(mate), base["sum_r"] + group * 2 + i, edge, columns
             )
             for i in range(2)
         ]
-        started.extend((edge, copy) for copy in far_sum)
-        mate_sum = pltpu.make_async_remote_copy(
-            src_ref=z_send.at[chunk, 2],
-            dst_ref=m_got.at[chunk],
-            send_sem=send_sem.at[len(started)],
-            recv_sem=recv_sem.at[base["sum_m"] + chunk],
-            device_id=line(mate),
-            device_id_type=mesh_id,
-        )
-        started.append((None, mate_sum))
+        own_sum = sum_copy(2, m_got, line(mate), base["sum_m"] + group, None, columns)
         across = [
-            pltpu.make_async_remote_copy(
-                src_ref=z_send.at[chunk, i],
-                dst_ref=f_got.at[chunk],
-                send_sem=send_sem.at[len(started) + i],
-                recv_sem=recv_sem.at[base["sum_f"] + chunk],
-                device_id=line(units[i]),
-                device_id_type=mesh_id,
-            )
+            sum_copy(i, f_got, line(units[i]), base["sum_f"] + group, inner, columns)
             for i in range(2)
         ]
-        started.extend((inner, copy) for copy in across)
+
+        def mate_part():
+            z_send[2, :, columns] = pair(group, columns, 2).astype(bf16)
+            own_sum.start()
 
         def edge_part():
             for i in range(2):
-                z_send[chunk, i] = pair(chunk, i).astype(bf16)
-                far_sum[i].start()
-            z_send[chunk, 2] = pair(chunk, 2).astype(bf16)
-            mate_sum.start()
+                z_send[i, :, columns] = pair(group, columns, i).astype(bf16)
+                near[i].start()
+            mate_part()
 
         def inner_part():
-            z_send[chunk, 2] = pair(chunk, 2).astype(bf16)
-            mate_sum.start()
             for i in range(2):
-                value = pair(chunk, i)
-                arrive(r_got.at[chunk, i], base["sum_r"] + chunk * 2 + i)
-                z_send[chunk, i] = (value + r_got[chunk, i].astype(f32)).astype(bf16)
+                value = pair(group, columns, i)
+                got = r_got.at[i, :, columns]
+                arrive(got, base["sum_r"] + group * 2 + i)
+                z_send[i, :, columns] = (value + got[...].astype(f32)).astype(bf16)
                 across[i].start()
-
-        pl.when(edge)(edge_part)
-        pl.when(inner)(inner_part)
-
-    def finish(chunk):
-        value = pair(chunk, 3)
-        arrive(m_got.at[chunk], base["sum_m"] + chunk)
-        value = value + m_got[chunk].astype(f32)
-        arrive(f_got.at[chunk], base["sum_f"] + chunk)
-        value = value + f_got[chunk].astype(f32)
-        for j, at in enumerate(groups[chunk]):
-            ffn_ref[:, at * span : (at + 1) * span] = value[:, j * span : (j + 1) * span]
+            mate_part()
+
+        return edge_part, inner_part
+
+    def finish(group, columns):
+        value = pair(group, columns, 3)
+        arrive(m_got.at[:, columns], base["sum_m"] + group)
+        value = value + m_got[:, columns].astype(f32)
+        arrive(f_got.at[:, columns], base["sum_f"] + group)
+        ffn_ref[:, columns] = value + f_got[:, columns].astype(f32)
 
     for i, at in enumerate((z, gate, outer, mate)):
         for c in range(row_chunks):
             arrive(row_piece(1, at, c), base["row_x"] + i * row_chunks + c)
     raise_rows(1)
     own[1].wait()
-    down_in_z(gate)
+    down_in_y(early)
+    made = [lower_edge(early, 0), lower_edge(early, 1)]
+    down_in_z(gate, inner)
     down_in_y(1)
     down_in_y(2)
-    lower(0)
+    made.append(lower_middle())
+    steps_of = [combine(*item) for item in made]
+    pl.when(edge)(steps_of[0][0])
+    pl.when(edge)(steps_of[1][0])
     down_in_z(outer)
-    down_in_y(0)
-    down_in_y(3)
-    lower(1)
-    gather_sums(0)
-    gather_sums(1)
-    finish(0)
-    finish(1)
+    made.append(lower_edge(late, 0))
+    steps_of.append(combine(*made[3]))
+    pl.when(edge)(steps_of[2][0])
+    down_in_y(late)
+    made.append(lower_edge(late, 1))
+    steps_of.append(combine(*made[4]))
+    for item in steps_of[:3]:
+        pl.when(inner)(item[1])
+    for item in steps_of[3:]:
+        pl.when(edge)(item[0])
+        pl.when(inner)(item[1])
+    finish(*made[2])
+    for at, flipped in ((early, 0), (early, 1), (late, 0), (late, 1)):
+        side = (1 - y) if flipped else y
+        finish(
+            1 + 2 * (at // (lines - 1)) + flipped,
+            columns_of((at * cols + side) * deep_part, deep_part),
+        )
     out_ref[...] = (mixed.astype(f32) + rms_scale(ffn_ref[...], last_ref[...])).astype(bf16)
     for cond, copy in started:
         if cond is None:
@@ -837,9 +871,8 @@
     slice_width = up_weight.shape[1] // lines
     vmem = pl.BlockSpec(memory_space=pltpu.VMEM)
     anywhere = pl.BlockSpec(memory_space=pl.ANY)
-    chunks = 2
+    chunks = 5
     heads = broad_width // DB + narrow_width // DN
-    chunk_width = deep // chunks
     _, sems = sem_layout(lines, tp, chunks, share_rows // 16)
     f32 = jnp.float32
     return pl.pallas_call(
@@ -863,13 +896,13 @@
             pltpu.VMEM((2, lines, cols, down_weight.shape[0], slice_width), bf16),
             pltpu.VMEM((2, lines, share_rows, deep), bf16),
             pltpu.VMEM((2 * lines * share_rows, 2 * slice_width), bf16),
-            pltpu.VMEM((chunks, lines, share_rows, chunk_width), f32),
-            pltpu.VMEM((chunks, lines, share_rows, chunk_width), bf16),
-            pltpu.VMEM((chunks, lines, share_rows, chunk_width), bf16),
-            pltpu.VMEM((chunks, 3, share_rows, chunk_width), bf16),
-            pltpu.VMEM((chunks, 2, share_rows, chunk_width), bf16),
-            pltpu.VMEM((chunks, share_rows, chunk_width), bf16),
-            pltpu.VMEM((chunks, share_rows, chunk_width), bf16),
+            pltpu.VMEM((lines, share_rows, deep), f32),
+            pltpu.VMEM((lines, share_rows, deep), bf16),
+            pltpu.VMEM((lines, share_rows, deep), bf16),
+            pltpu.VMEM((3, share_rows, deep), bf16),
+            pltpu.VMEM((2, share_rows, deep), bf16),
+            pltpu.VMEM((share_rows, deep), bf16),
+            pltpu.VMEM((share_rows, deep), bf16),
             pltpu.VMEM((share_rows, deep), f32),
             pltpu.SemaphoreType.DMA((2 * sems,)),
             pltpu.SemaphoreType.DMA((sems,)),

time: 110 us -> 102 us (0.927)
  Pallas kernels: 105 us -> 97.8 us
    pallas_call x1, Pallas kernels: 105 us -> 97.8 us  [fast_local(): pl.pallas_call(functools.partial(layer_kernel, sp, tp), out_shape=jax.Sha...]
where the time goes in v3:
time: 102 us
  Pallas kernels  97.8 us (96%)
  local copies, waits for them, and re-layouts  3.09 us (3%)
  other arithmetic  1.23 us (1%)
    pallas_call x1, Pallas kernels, fast_local(): pl.pallas_call(functools.partial(layer_kernel, sp, tp), out_shape=jax.Sha...  97.8 us
    unnamed x2, local copies, waits for them, and re-layouts  3.09 us

profile of v3, /device:TPU:0, one launch (start us, length us, event | category | flops | bytes accessed | tf_op | source)
XLA Modules:
  0.0 102.2 jit_solution(14787898889044400806)
XLA Ops:
  0.0 0.4 multiply_cosine_fusion
  0.4 0.8 pad_maximum_fusion.table_ref
  1.2 1.5 %copy.20.key_rope_ref = bf16[192,64]{1,0:T(8,128)(2,1)} copy(bf16[192,64]{0,1:T(8,128)(2,1)} %param.21) | data formatting | bytes 49152 | tf_op args[4]
  2.7 97.8 %shard_map.163 = bf16[48,2048]{1,0:T(8,128)(2,1)} custom-call(bf16[192,512]{1,0:T(8,128)(2,1)} %latent_ref.1, bf16[192,64]{1,0:T(8,128)(2,1)} %copy.20.key_rope_ref, f32[192,128]{1,0:T(8,128)} %pad_maximum_fusion.table_ref, f32[1,512]{1,0:T(1,128)} %bitcast.7, bf16[192,384]{1,0:T(8,128)(2,1)} %qb_in.1, bf16[192,256]{1,0:T(8,128)(2,1)} %qn_in.1, ...), custom_call_target="tpu_custom_call" | custom-call | tf_op jit(solution)/shard_map/pallas_call | solution.py:878
  100.5 1.6 %copy.22 = bf16[48,2048]{1,0:T(8,128)(2,1)} copy(bf16[48,2048]{1,0:T(8,128)(2,1)} %shard_map.163) | data formatting | bytes 393216
  (2 shorter events, 0.0 us)

commit v4 on v3

--- a/solution.py
+++ b/solution.py
@@ -3,6 +3,7 @@
 
 import jax
 import jax.numpy as jnp
+import numpy as np
 from jax import lax
 from jax.experimental import pallas as pl
 from jax.experimental.pallas import tpu as pltpu
@@ -241,15 +242,15 @@
     tp,
     latent_ref,
     key_rope_ref,
-    table_ref,
+    frequency_ref,
     latent_gain_ref,
-    qb_in,
-    qn_in,
-    resid_ref,
-    kb_ref,
-    vb_ref,
-    kn_ref,
-    vn_ref,
+    qb_hbm,
+    qn_hbm,
+    resid_hbm,
+    kb_hbm,
+    vb_hbm,
+    kn_hbm,
+    vn_hbm,
     ob_hbm,
     on_hbm,
     post_ref,
@@ -258,6 +259,13 @@
     up_hbm,
     down_hbm,
     out_ref,
+    qb_in,
+    qn_in,
+    resid_ref,
+    kb_ref,
+    vb_ref,
+    kn_ref,
+    vn_ref,
     mine_ref,
     qb_ref,
     qn_ref,
@@ -307,8 +315,8 @@
     edge = (z == 0) | (z == 3)
     bf16 = jnp.bfloat16
     f32 = jnp.float32
-    share = resid_ref.shape[0] // tp
-    block_rows = resid_ref.shape[0]
+    block_rows = latent_ref.shape[0]
+    share = block_rows // tp
     width = up.shape[3]
     row_step = 16
     row_chunks = share // row_step
@@ -323,20 +331,44 @@
     for peer in peers:
         pl.semaphore_signal(barrier, inc=1, device_id=peer, device_id_type=mesh_id)
 
-    rope = key_rope_ref.shape[1]
+    locals_ = []
+
+    def bring(src, dst):
+        copy = pltpu.make_async_copy(src, dst, local_sem.at[len(locals_)])
+        copy.start()
+        locals_.append(copy)
+        return copy
+
+    rope = key_rope_ref.shape[0]
     half_rope = rope // 2
 
-    def turn(values, table):
+    def table(first, count):
+        row = lax.broadcasted_iota(jnp.int32, (count, rope), 0) + first
+        angles = row.astype(f32) * frequency_ref[...]
+        lane = lax.broadcasted_iota(jnp.int32, (count, rope), 1)
+        sine = jnp.sin(angles)
+        return jnp.cos(angles), jnp.where(lane < half_rope, -sine, sine)
+
+    def turn(values, tables):
         values = values.astype(f32)
         swapped = jnp.concatenate([values[:, half_rope:], values[:, :half_rope]], axis=1)
-        return (values * table[:, :rope] + swapped * table[:, rope:]).astype(bf16)
+        return (values * tables[0] + swapped * tables[1]).astype(bf16)
 
     latent_width = latent_ref.shape[1]
     mine_rows = pl.ds(pl.multiple_of(t * share, 16), share)
     mine_ref[:, :latent_width] = rms_scale(
         latent_ref[mine_rows, :].astype(f32), latent_gain_ref[...]
     ).astype(bf16)
-    mine_ref[:, latent_width:] = turn(key_rope_ref[mine_rows, :], table_ref[mine_rows, :])
+    picked = lax.broadcasted_iota(jnp.int32, (share, block_rows), 1) == (
+        lax.broadcasted_iota(jnp.int32, (share, block_rows), 0) + t * share
+    )
+    key_rows = lax.dot_general(
+        jnp.where(picked, 1.0, 0.0).astype(bf16),
+        key_rope_ref[...],
+        (((1,), (1,)), ((), ())),
+        preferred_element_type=f32,
+    )
+    mine_ref[:, latent_width:] = turn(key_rows, table(s * block_rows + t * share, share))
     pl.semaphore_wait(barrier, len(peers))
 
     started = []
@@ -366,14 +398,6 @@
             device_id_type=mesh_id,
         ).wait_recv()
 
-    locals_ = []
-
-    def bring(src, dst):
-        copy = pltpu.make_async_copy(src, dst, local_sem.at[len(locals_)])
-        copy.start()
-        locals_.append(copy)
-        return copy
-
     def block(k, flipped):
         return (z - k) * cols + ((1 - y) if flipped else y)
 
@@ -419,7 +443,17 @@
     send_down(gate, z == 2)
     own = [bring(cut(up_hbm, z), up_at(core, s))]
     own.append(bring(cut(down_hbm, z), down_at(core, z)))
-    outs = [bring(ob_hbm, ob), bring(on_hbm, on)]
+    queries = [bring(qb_hbm, qb_in), bring(qn_hbm, qn_in)]
+    expands = [
+        bring(kb_hbm, kb_ref),
+        bring(vb_hbm, vb_ref),
+        bring(kn_hbm, kn_ref),
+        bring(vn_hbm, vn_ref),
+    ]
+    outs = [bring(ob_hbm, ob), bring(on_hbm, on), bring(resid_hbm, resid_ref)]
+    query_table = table(s * block_rows, block_rows)
+    for copy in queries:
+        copy.wait()
 
     for queries, turned, size in ((qb_in, qb_ref, DB), (qn_in, qn_ref, DN)):
         step = size + rope
@@ -427,7 +461,7 @@
             middle = h * step + size
             turned[:, h * step : middle] = queries[:, h * step : middle]
             turned[:, middle : middle + rope] = turn(
-                queries[:, middle : middle + rope], table_ref[...]
+                queries[:, middle : middle + rope], query_table
             )
 
     def when(k):
@@ -536,6 +570,8 @@
     send(cut(up_hbm, z), up_at(core, s), peer_y, base["up_y"])
     send(cut(up_hbm, z), up_at(core, s), peer_c, base["up_c"])
     own_copy.wait()
+    for copy in expands:
+        copy.wait()
     attend(0)
     lat_in_y(1)
     lat_in_y(2)
@@ -640,6 +676,8 @@
     steps = (z,) + far
     down_in_z(mate, inner)
     down_in_z(gate, edge)
+    send_down(gate, z == 0)
+    send_down(outer, edge)
     for i, at in enumerate(steps):
         up_in_y(i, at)
     own[0].wait()
@@ -660,8 +698,6 @@
             ] = jnp.square(jnp.maximum(product, 0.0)).astype(bf16)
 
     raise_rows(0)
-    send_down(gate, z == 0)
-    send_down(outer, edge)
 
     def down_in_y(at):
         for i in range(2):
@@ -849,20 +885,13 @@
     tp = lax.axis_size("tp")
     cols = row_parts
     lines = sp // cols
-    s = lax.axis_index("sp")
-    z = s // cols
-    y = s % cols
     local_rows = resid.shape[0]
     share_rows = local_rows // tp
-    query_pos = s * local_rows + jnp.arange(local_rows, dtype=jnp.int32)
     rope_width = key_rope.shape[1]
     bf16 = jnp.bfloat16
 
-    frequency = rope_base ** (-2.0 * jnp.arange(rope_width // 2, dtype=jnp.float32) / rope_width)
-    angles = query_pos.astype(jnp.float32)[:, None] * frequency[None, :]
-    cosine, sine = jnp.cos(angles), jnp.sin(angles)
-    table = jnp.concatenate([cosine, cosine, -sine, sine], axis=1)
-    half_rows = local_rows // 2
+    steps = np.arange(rope_width, dtype=np.float32) % (rope_width // 2)
+    frequency = np.power(np.float32(rope_base), -2.0 * steps / rope_width).astype(np.float32)[None]
     both_width = latent.shape[1] + rope_width
     broad_width = key_up_broad.shape[1]
     narrow_width = key_up_narrow.shape[1]
@@ -878,9 +907,16 @@
     return pl.pallas_call(
         functools.partial(layer_kernel, sp, tp),
         out_shape=jax.ShapeDtypeStruct((share_rows, deep), bf16),
-        in_specs=[vmem] * 11 + [anywhere] * 2 + [vmem] * 3 + [anywhere] * 2,
+        in_specs=[vmem] * 4 + [anywhere] * 9 + [vmem] * 3 + [anywhere] * 2,
         out_specs=vmem,
         scratch_shapes=[
+            pltpu.VMEM(query_broad.shape, bf16),
+            pltpu.VMEM(query_narrow.shape, bf16),
+            pltpu.VMEM(resid.shape, bf16),
+            pltpu.VMEM(key_up_broad.shape, bf16),
+            pltpu.VMEM(value_up_broad.shape, bf16),
+            pltpu.VMEM(key_up_narrow.shape, bf16),
+            pltpu.VMEM(value_up_narrow.shape, bf16),
             pltpu.VMEM((share_rows, both_width), bf16),
             pltpu.VMEM(query_broad.shape, bf16),
             pltpu.VMEM(query_narrow.shape, bf16),
@@ -906,7 +942,7 @@
             pltpu.VMEM((share_rows, deep), f32),
             pltpu.SemaphoreType.DMA((2 * sems,)),
             pltpu.SemaphoreType.DMA((sems,)),
-            pltpu.SemaphoreType.DMA((5,)),
+            pltpu.SemaphoreType.DMA((12,)),
             pltpu.SemaphoreType.REGULAR,
         ],
         compiler_params=pltpu.CompilerParams(
@@ -914,8 +950,8 @@
         ),
     )(
         latent,
-        key_rope,
-        table,
+        key_rope.T,
+        frequency,
         latent_gain[None],
         query_broad,
         query_narrow,

time: 102 us -> 95.4 us (0.935)
  Pallas kernels: 97.8 us -> 93.6 us
  local copies, waits for them, and re-layouts: 3.09 us -> 1.62 us
  other arithmetic: 1.23 us -> 0 us
    pallas_call x1, Pallas kernels: 97.8 us -> 93.6 us  [fast_local(): pl.pallas_call(functools.partial(layer_kernel, sp, tp), out_shape=jax.Sha...]
    unnamed x2 -> x1, local copies, waits for them, and re-layouts: 3.09 us -> 1.62 us
where the time goes in v4:
time: 95.4 us; the launch traced here: 95.3 us
  Pallas kernels  93.6 us (98%)
  local copies, waits for them, and re-layouts  1.62 us (2%)
    pallas_call x1, Pallas kernels, fast_local(): pl.pallas_call(functools.partial(layer_kernel, sp, tp), out_shape=jax.Sha...  93.6 us

profile of v4, /device:TPU:0, one launch (start us, length us, event | category | flops | bytes accessed | tf_op | source)
XLA Modules:
  0.0 95.3 jit_solution(2871478218284381815)
XLA Ops:
  0.0 93.6 %shard_map.172 = bf16[48,2048]{1,0:T(8,128)(2,1)} custom-call(bf16[192,512]{1,0:T(8,128)(2,1)} %latent_ref.1, bf16[64,192]{1,0:T(8,128)(2,1)} %bitcast.5, f32[1,64]{1,0:T(1,128)} %constant.2.clone.frequency_ref, f32[1,512]{1,0:T(1,128)} %bitcast.9, bf16[192,384]{1,0:T(8,128)(2,1)} %qb_hbm.1, bf16[192,256]{1,0:T(8,128)(2,1)} %qn_hbm.1, ...), custom_call_target="tpu_custom_call" | custom-call | tf_op jit(solution)/shard_map/pallas_call | solution.py:907
  93.6 1.6 %copy.20 = bf16[48,2048]{1,0:T(8,128)(2,1)} copy(bf16[48,2048]{1,0:T(8,128)(2,1)} %shard_map.172) | data formatting | bytes 393216

commit v5 on v4

--- a/solution.py
+++ b/solution.py
@@ -705,7 +705,7 @@
             arrive(held, base["down_y"] + 2 * at + i)
             send(held, held, peer_c, base["down_c"] + 4 * at + 2 + i)
 
-    units = (gate, outer, mate, z)
+    units = (outer, gate, mate, z)
 
     deep_part = down.shape[3]
     early = (lines - 1) * half

time: 95.4 us -> 95.1 us (level)
  no operation moved by 1% of the time
where the time goes in v5:
time: 95.1 us; the launch traced here: 94.9 us
  Pallas kernels  93.3 us (98%)
  local copies, waits for them, and re-layouts  1.62 us (2%)
    pallas_call x1, Pallas kernels, fast_local(): pl.pallas_call(functools.partial(layer_kernel, sp, tp), out_shape=jax.Sha...  93.3 us

profile of v5, /device:TPU:0, one launch (start us, length us, event | category | flops | bytes accessed | tf_op | source)
XLA Modules:
  0.0 94.9 jit_solution(10404895717508637409)
XLA Ops:
  0.0 93.3 %shard_map.172 = bf16[48,2048]{1,0:T(8,128)(2,1)} custom-call(bf16[192,512]{1,0:T(8,128)(2,1)} %latent_ref.1, bf16[64,192]{1,0:T(8,128)(2,1)} %bitcast.5, f32[1,64]{1,0:T(1,128)} %constant.2.clone.frequency_ref, f32[1,512]{1,0:T(1,128)} %bitcast.9, bf16[192,384]{1,0:T(8,128)(2,1)} %qb_hbm.1, bf16[192,256]{1,0:T(8,128)(2,1)} %qn_hbm.1, ...), custom_call_target="tpu_custom_call" | custom-call | tf_op jit(solution)/shard_map/pallas_call | solution.py:907
  93.3 1.6 %copy.20 = bf16[48,2048]{1,0:T(8,128)(2,1)} copy(bf16[48,2048]{1,0:T(8,128)(2,1)} %shard_map.172) | data formatting | bytes 393216
